TPU v7x, 32 devices: a whole 2x2x4 slice. The times are simulated.
32 devices in a mesh: grp: 2 (over y), fs: 4 (over z), tp: 4 (over x, core).
Axes of the slice: x: 2, y: 2, z: 4, core: 2. Of those that a mesh axis runs over, the one named last changes fastest.
Arguments:
- tokens: bfloat16 [3072, 2048], P(('grp', 'fs')), parts along dimension 0, may hold values from -3 to 3
- gate_weight: bfloat16 [2048, 5120], P('fs', 'tp'), may hold values from -0.125 to 0.125
- up_weight: bfloat16 [2048, 5120], P('fs', 'tp'), may hold values from -0.125 to 0.125
- down_weight: bfloat16 [5120, 2048], P('tp', 'fs'), may hold values from -0.078125 to 0.078125
- pool_weight: bfloat16 [512, 4, 512], P('fs', None, 'tp'), may hold values from -0.375 to 0.375
- pool_bias: float32 [4, 512], replicated, may hold values from -3 to 3
- pool_scale: float32 [2048], replicated, may hold values from 0.1 to 1.9
- gain_first: float32 [2048], replicated, may hold values from 0.1 to 1.9
- gain_mix: float32 [2048], replicated, may hold values from 0.1 to 1.9
- gain_second: float32 [2048], replicated, may hold values from 0.1 to 1.9
Outputs:
- result: bfloat16 [3072, 2048], P(('grp', 'fs')), parts along dimension 0
There are 2 independent parts, one for each index of `grp`. A program takes and returns all parts, laid end to end along the dimension named above; an argument that names none is the same for every part. Nothing has to cross between parts.
All inputs are finite; a program needn't handle non-finite values.
Results may differ from a plain program's by a relative error of at most 0.018.
Values may be sent and summed in bfloat16 or wider, within the bound.
A program may use at most 64 MiB of HBM per device.

v0:
```python
import functools

import jax
import jax.numpy as jnp
from jax import lax
from jax.experimental import pallas as pl
from jax.experimental.pallas import tpu as pltpu
from jax.sharding import PartitionSpec as P

eps = 1e-06
pool_spans = (2, 4, 8, 16)
pad_width = 8
MESH = pl.DeviceIdType.MESH


def rms_scale(values, gain_vec):
    fvalues = values.astype(jnp.float32)
    scaled = fvalues * lax.rsqrt(jnp.mean(fvalues * fvalues, axis=-1, keepdims=True) + eps)
    return (scaled * gain_vec).astype(jnp.bfloat16)


def ffn_hidden(normed, gate_full, up_full):
    gate_proj = jnp.dot(normed, gate_full, preferred_element_type=jnp.float32)
    up_proj = jnp.dot(normed, up_full, preferred_element_type=jnp.float32)
    return (jax.nn.silu(gate_proj) * up_proj).astype(jnp.bfloat16)


def pool_block(padded, offset, seq_len, pool_full, pool_bias, pool_scale):
    n_tokens = padded.shape[0] - 2 * pad_width
    group_width = pool_full.shape[0]
    position = offset + lax.iota(jnp.int32, n_tokens)
    column_pos = offset - pad_width + lax.iota(jnp.int32, padded.shape[0])
    center = padded[pad_width : pad_width + n_tokens].astype(jnp.float32)
    outputs = []
    for group_number, window_span in enumerate(pool_spans):
        low_edge = jnp.clip(position - window_span // 2, 0, seq_len)
        high_edge = jnp.clip(position - window_span // 2 + window_span, 0, seq_len)
        band_mask = (
            (column_pos[None, :] >= low_edge[:, None]) & (column_pos[None, :] < high_edge[:, None])
        ).astype(jnp.bfloat16)
        lower_col = group_number * group_width
        columns = padded[:, lower_col : lower_col + group_width]
        window_sum = jnp.dot(band_mask, columns, preferred_element_type=jnp.float32)
        window_mean = window_sum / (high_edge - low_edge).astype(jnp.float32)[:, None]
        deviation = (window_mean - center[:, lower_col : lower_col + group_width]).astype(
            jnp.bfloat16
        )
        mapped = jnp.dot(
            deviation, pool_full[:, group_number, :], preferred_element_type=jnp.float32
        )
        outputs.append(mapped + pool_bias[group_number])
    return jnp.concatenate(outputs, axis=-1) * pool_scale


def shards(
    tokens,
    gate_weight,
    up_weight,
    down_weight,
    pool_weight,
    pool_bias,
    pool_scale,
    gain_first,
    gain_mix,
    gain_second,
):
    gate_full, up_full, pool_half = (
        lax.all_gather(gate_weight, "fs", axis=0, tiled=True),
        lax.all_gather(up_weight, "fs", axis=0, tiled=True),
        lax.all_gather(pool_weight, "fs", axis=0, tiled=True),
    )
    down_full = lax.all_gather(down_weight, "fs", axis=1, tiled=True)
    pool_full = lax.all_gather(pool_half, "tp", axis=2, tiled=True)
    seq_len = tokens.shape[0]
    first_normed = rms_scale(tokens, gain_first)
    first_hidden = ffn_hidden(first_normed, gate_full, up_full)
    second_gate, second_up, second_down = (gate_full, up_full, down_full)
    first_branch = lax.psum(
        jnp.dot(first_hidden, down_full, preferred_element_type=jnp.float32).astype(jnp.bfloat16),
        "tp",
    ).astype(jnp.float32)
    after_first = (tokens.astype(jnp.float32) + 0.5 * first_branch).astype(jnp.bfloat16)
    mix_normed = rms_scale(after_first, gain_mix)
    padded = jnp.pad(mix_normed, ((pad_width, pad_width), (0, 0)))
    mixed = pool_block(padded, 0, seq_len, pool_full, pool_bias, pool_scale)
    after_mix = (after_first.astype(jnp.float32) + mixed).astype(jnp.bfloat16)
    second_normed = rms_scale(after_mix, gain_second)
    second_hidden = ffn_hidden(second_normed, second_gate, second_up)
    second_branch = lax.psum(
        jnp.dot(second_hidden, second_down, preferred_element_type=jnp.float32).astype(
            jnp.bfloat16
        ),
        "tp",
    ).astype(jnp.float32)
    return (after_mix.astype(jnp.float32) + 0.5 * second_branch).astype(jnp.bfloat16)


def fused_kernel(
    sizes, tok_ref, gate_ref, up_ref, down_ref, pool_ref, bias_ref, scale_ref, gain1_ref, gainm_ref, gain2_ref,
    out_ref,
    gu_full, down_full, pool_full, acc, normed, hidden, amix, res, part, rbuf, xs, xr,
    zsend, zleft, zrecv, ysend, yrecv, tsend, trecv, lsem, csend, crecv, xsend, xrecv, fsend, frecv, osem,
):
    n, n_tp = sizes
    g, z, t = lax.axis_index("grp"), lax.axis_index("fs"), lax.axis_index("tp")
    core = lax.rem(t, 2)
    y_peer, right, left = {"grp": 1 - g}, {"fs": z + 1}, {"fs": z - 1}
    mate, x_peer = {"tp": t + 1 - 2 * core}, {"tp": lax.rem(t + 2, n_tp)}
    n_rows, width = tok_ref.shape
    d_loc, f_loc = gate_ref.shape
    groups, pool_rows, pool_cols = pool_ref.shape
    half_rows = n_rows // 2
    block_cols = d_loc // 2
    f32 = jnp.float32

    def remote(src, dst, s_sem, r_sem, dev):
        return pltpu.make_async_remote_copy(
            src_ref=src, dst_ref=dst, send_sem=s_sem, recv_sem=r_sem, device_id=dev, device_id_type=MESH
        )

    barrier = pltpu.get_barrier_semaphore()

    def greet(dev):
        pl.semaphore_signal(barrier, inc=1, device_id=dev, device_id_type=MESH)

    greet(y_peer)
    for off in range(1, n_tp):
        greet({"tp": lax.rem(t + off, n_tp)})

    @pl.when(z > 0)
    def _():
        greet(left)

    @pl.when(z < n - 1)
    def _():
        greet(right)

    pl.semaphore_wait(barrier, n_tp + jnp.minimum(z, 1) + jnp.minimum(n - 1 - z, 1))

    pieces = [("pool", 0, 1)] + [(name, c, 4) for name in ("gate", "up", "down") for c in range(4)]
    n_pieces = len(pieces)

    def rows_of(name, half, c, count):
        if name == "down":
            return c * (f_loc // count), f_loc // count, f_loc
        total = {"pool": pool_rows, "gate": d_loc, "up": d_loc}[name]
        size = total // (2 * count)
        return half * (total // 2) + c * size, size, total

    def region(name, s, half, c, count):
        start, size, total = rows_of(name, half, c, count)
        if name == "down":
            return down_full.at[s, half, pl.ds(start, size), :]
        rows = pl.ds(pl.multiple_of(s * total + start, 16), size)
        if name == "pool":
            return pool_full.at[:, rows, pl.ds(pl.multiple_of(t * pool_cols, 128), pool_cols)]
        return gu_full.at[0 if name == "gate" else 1, rows, :]

    def source(name, half, c, count):
        start, size, _ = rows_of(name, half, c, count)
        if name == "down":
            return down_ref.at[pl.ds(start, size), pl.ds(pl.multiple_of(half * block_cols, 128), block_cols)]
        rows = pl.ds(pl.multiple_of(start, 16), size)
        if name == "pool":
            return pool_ref.at[:, rows, :]
        return {"gate": gate_ref, "up": up_ref}[name].at[rows, :]

    def own_right(k):
        name, c, count = pieces[k]
        return remote(source(name, g, c, count), region(name, z, g, c, count), zsend.at[z, k], zrecv.at[z, k], right)

    def own_left(k):
        name, c, count = pieces[k]
        return remote(source(name, g, c, count), region(name, z, g, c, count), zleft.at[k], zrecv.at[z, k], left)

    def pass_on(k, s, dev):
        name, c, count = pieces[k]
        there = region(name, s, g, c, count)
        return remote(there, there, zsend.at[s, k], zrecv.at[s, k], dev)

    def share(k, s, half):
        name, c, count = pieces[k]
        there = region(name, s, half, c, count)
        return remote(there, there, ysend.at[s, k], yrecv.at[s, k], y_peer)

    for k in range(n_pieces):

        @pl.when(z < n - 1)
        def _():
            own_right(k).start()

        @pl.when(z > 0)
        def _():
            own_left(k).start()

    own_rows = pl.ds(pl.multiple_of(z * d_loc, 128), d_loc)
    own_pool = pool_full.at[
        :, pl.ds(pl.multiple_of(z * pool_rows, 16), pool_rows), pl.ds(pl.multiple_of(t * pool_cols, 128), pool_cols)
    ]
    local = [
        pltpu.make_async_copy(pool_ref, own_pool, lsem.at[0]),
        pltpu.make_async_copy(gate_ref, gu_full.at[0, own_rows, :], lsem.at[1]),
        pltpu.make_async_copy(up_ref, gu_full.at[1, own_rows, :], lsem.at[2]),
        pltpu.make_async_copy(down_ref.at[:, pl.ds(0, block_cols)], down_full.at[z, 0], lsem.at[3]),
        pltpu.make_async_copy(down_ref.at[:, pl.ds(block_cols, block_cols)], down_full.at[z, 1], lsem.at[4]),
    ]
    for copy in local:
        copy.start()

    def norm_rows(src, gain):
        @pl.loop(0, n_rows // 32)
        def _(r):
            rows = pl.ds(pl.multiple_of(r * 32, 32), 32)
            values = src[rows, :].astype(f32)
            scaled = values * lax.rsqrt(jnp.mean(values * values, axis=-1, keepdims=True) + eps)
            normed[rows, :] = (scaled * gain[...]).astype(jnp.bfloat16)

    tile = 256

    def add_shard(w, s):
        k_cols = pl.ds(pl.multiple_of(s * d_loc, 128), d_loc)

        @pl.loop(0, f_loc // tile)
        def _(i):
            cols = pl.ds(pl.multiple_of(i * tile, tile), tile)
            acc[w, :, cols] += jnp.dot(normed[:, k_cols], gu_full[w, k_cols, cols], preferred_element_type=f32)

    def pool_copy(off, s, sender):
        cols = pl.ds(pl.multiple_of(sender * pool_cols, 128), pool_cols)
        there = pool_full.at[:, pl.ds(pl.multiple_of(s * pool_rows, 16), pool_rows), cols]
        return remote(there, there, tsend.at[off - 1, s], trecv.at[off - 1, s], {"tp": lax.rem(t + off, n_tp)})

    def spread_pool(s):
        for off in range(1, n_tp):
            pool_copy(off, s, t).start()

    norm_rows(tok_ref, gain1_ref)
    acc[...] = jnp.zeros_like(acc)
    for copy in local:
        copy.wait()
    spread_pool(z)

    @pl.loop(0, 2)
    def _(w):
        add_shard(w, z)

    def both_sides(d, act):
        @pl.when(z >= d)
        def _():
            act(z - d, z < n - 1, right)

        @pl.when(z + d < n)
        def _():
            act(z + d, z > 0, left)

    def relay(name, d, only=None):
        for k in range(n_pieces):
            if pieces[k][0] != name or only not in (None, pieces[k][1]):
                continue

            def act(s, more, dev):
                pass_on(k, s, dev).wait_recv()

                @pl.when(more)
                def _():
                    pass_on(k, s, dev).start()

                share(k, s, g).start()

            both_sides(d, act)

    def settle(name, s):
        for k in range(n_pieces):
            if pieces[k][0] == name:
                share(k, s, 1 - g).wait_recv()

    def settle_pool(s, *_):
        settle("pool", s)
        spread_pool(s)

    def settle_gate(s, *_):
        settle("gate", s)
        add_shard(0, s)

    def settle_up(s, *_):
        settle("up", s)
        add_shard(1, s)

    @pl.loop(1, n - 1)
    def _(d):
        relay("pool", d)
        relay("gate", d)
        both_sides(d, settle_pool)
        relay("up", d)
        both_sides(d, settle_gate)
        relay("down", d)
        both_sides(d, settle_up)

    relay("pool", n - 1)
    relay("gate", n - 1)
    both_sides(n - 1, settle_pool)
    relay("up", n - 1)
    both_sides(n - 1, settle_gate)
    both_sides(n - 1, settle_up)
    relay("down", n - 1, 0)

    def activate(gate_proj, up_proj):
        return (gate_proj / (1.0 + jnp.exp(-gate_proj)) * up_proj).astype(jnp.bfloat16)

    @pl.loop(0, f_loc // tile)
    def _(i):
        cols = pl.ds(pl.multiple_of(i * tile, tile), tile)
        hidden[:, cols] = activate(acc[0, :, cols], acc[1, :, cols])

    turn = 1 - 2 * ((2 * z) // n)
    mine = pl.ds(pl.multiple_of(core * half_rows, 16), half_rows)
    other = pl.ds(pl.multiple_of((1 - core) * half_rows, 16), half_rows)

    n_blocks = 2 * n

    def branch_sum(phase, base):
        def place(j):
            return lax.rem(z + turn * (j // 2) + n, n), g if j % 2 == 0 else 1 - g

        def columns(j):
            s, half = place(j)
            return pl.ds(pl.multiple_of(s * d_loc + half * block_cols, 128), block_cols)

        def pair_copy(j):
            return remote(part.at[phase, j, other, :], rbuf.at[phase, j], csend.at[phase, j], crecv.at[phase, j], mate)

        def x_copy(j):
            return remote(xs.at[phase, j], xr.at[phase, j], xsend.at[phase, j], xrecv.at[phase, j], x_peer)

        def final_copy(j, rows):
            there = res.at[phase, rows, columns(j)]
            return remote(there, there, fsend.at[phase, j], frecv.at[phase, j], mate)

        def multiply(j):
            s, half = place(j)
            if phase == 0 and j in (1, 3, 5):
                relay("down", n - 1, (j + 1) // 2)
            if phase == 0 and j >= 2 and j % 2 == 1:
                settle("down", s)
            part[phase, j] = jnp.dot(
                hidden[...], down_full[s, half], preferred_element_type=f32
            ).astype(jnp.bfloat16)
            pair_copy(j).start()

        def add_pair(j):
            pair_copy(j).wait_recv()
            xs[phase, j] = (part[phase, j, mine, :].astype(f32) + rbuf[phase, j].astype(f32)).astype(jnp.bfloat16)
            x_copy(j).start()

        def finish(j):
            x_copy(j).wait_recv()
            total = xs[phase, j].astype(f32) + xr[phase, j].astype(f32)
            cols = columns(j)
            res[phase, mine, cols] = (base[mine, cols].astype(f32) + 0.5 * total).astype(jnp.bfloat16)
            final_copy(j, mine).start()

        early = n_blocks // 2 if phase == 0 else 0
        for j in range(n_blocks + 1):
            if j == n_blocks - 1:
                for done in range(early):
                    finish(done)
            if j < n_blocks:
                multiply(j)
            if j > 0:
                add_pair(j - 1)
        for j in range(early, n_blocks):
            finish(j)
        for j in range(n_blocks):
            final_copy(j, other).wait_recv()

        def drain():
            for j in range(n_blocks):
                pair_copy(j).wait_send()
                x_copy(j).wait_send()
                final_copy(j, mine).wait_send()

        return drain

    drain_first = branch_sum(0, tok_ref)

    norm_rows(res.at[0], gainm_ref)
    for off in range(1, n_tp):
        for s in range(n):
            pool_copy(off, s, lax.rem(t - off + n_tp, n_tp)).wait_recv()
    group_width = width // groups
    row_id = lax.broadcasted_iota(jnp.int32, (n_rows, n_rows), 0)
    col_id = lax.broadcasted_iota(jnp.int32, (n_rows, n_rows), 1)
    position = lax.broadcasted_iota(jnp.int32, (n_rows, 1), 0)
    for k, span in enumerate(pool_spans):
        low = row_id - span // 2
        band = jnp.where((col_id >= low) & (col_id < low + span), 1.0, 0.0).astype(jnp.bfloat16)
        first = jnp.maximum(position - span // 2, 0)
        last = jnp.minimum(position - span // 2 + span, n_rows)
        inverse = 1.0 / (last - first).astype(f32)
        cols = pl.ds(k * group_width, group_width)
        mean = jnp.dot(band, normed[:, cols], preferred_element_type=f32) * inverse
        deviation = (mean - normed[:, cols].astype(f32)).astype(jnp.bfloat16)
        mapped = jnp.dot(deviation, pool_full[k], preferred_element_type=f32) + bias_ref[pl.ds(k, 1), :]
        amix[:, cols] = (res[0, :, cols].astype(f32) + mapped * scale_ref[:, cols]).astype(jnp.bfloat16)

    norm_rows(amix, gain2_ref)

    @pl.loop(0, f_loc // tile)
    def _(i):
        cols = pl.ds(pl.multiple_of(i * tile, tile), tile)
        gate_proj = jnp.dot(normed[...], gu_full[0, :, cols], preferred_element_type=f32)
        up_proj = jnp.dot(normed[...], gu_full[1, :, cols], preferred_element_type=f32)
        hidden[:, cols] = activate(gate_proj, up_proj)

    drain_second = branch_sum(1, amix)
    out_copy = pltpu.make_async_copy(res.at[1], out_ref, osem)
    out_copy.start()

    for k in range(n_pieces):

        @pl.when(z < n - 1)
        def _():
            own_right(k).wait_send()

        @pl.when(z > 0)
        def _():
            own_left(k).wait_send()

    @pl.loop(1, n)
    def _(d):
        for k in range(n_pieces):

            def act(s, more, dev):
                @pl.when(more)
                def _():
                    pass_on(k, s, dev).wait_send()

                share(k, s, g).wait_send()

            both_sides(d, act)

    @pl.loop(0, n)
    def _(s):
        for off in range(1, n_tp):
            pool_copy(off, s, t).wait_send()

    drain_first()
    drain_second()
    out_copy.wait()


def fused_shards(
    n, n_tp, tokens, gate_weight, up_weight, down_weight, pool_weight, pool_bias, pool_scale,
    gain_first, gain_mix, gain_second,
):
    n_rows, width = tokens.shape
    d_loc, f_loc = gate_weight.shape
    groups = pool_weight.shape[1]
    pool = jnp.swapaxes(pool_weight, 0, 1)
    bf16, dma, vmem = jnp.bfloat16, pltpu.SemaphoreType.DMA, pltpu.VMEM
    in_vmem, anywhere = pl.BlockSpec(memory_space=pltpu.VMEM), pl.BlockSpec(memory_space=pl.ANY)
    half = n_rows // 2
    return pl.pallas_call(
        functools.partial(fused_kernel, (n, n_tp)),
        out_shape=jax.ShapeDtypeStruct((n_rows, width), bf16),
        in_specs=[in_vmem] + [anywhere] * 4 + [in_vmem] * 5,
        out_specs=anywhere,
        scratch_shapes=[
            vmem((2, n * d_loc, f_loc), bf16),
            vmem((n, 2, f_loc, d_loc // 2), bf16),
            vmem((groups, n * pool.shape[1], n_tp * pool.shape[2]), bf16),
            vmem((2, n_rows, f_loc), jnp.float32),
            vmem((n_rows, width), bf16),
            vmem((n_rows, f_loc), bf16),
            vmem((n_rows, width), bf16),
            vmem((2, n_rows, width), bf16),
            vmem((2, 2 * n, n_rows, d_loc // 2), bf16),
            vmem((2, 2 * n, half, d_loc // 2), bf16),
            vmem((2, 2 * n, half, d_loc // 2), bf16),
            vmem((2, 2 * n, half, d_loc // 2), bf16),
            dma((n, 13)), dma((13,)), dma((n, 13)), dma((n, 13)), dma((n, 13)),
            dma((n_tp - 1, n)), dma((n_tp - 1, n)), dma((5,)),
            *[dma((2, 2 * n))] * 6, dma,
        ],
        compiler_params=pltpu.CompilerParams(
            collective_id=0, has_side_effects=True, vmem_limit_bytes=60 * 1024 * 1024
        ),
    )(
        tokens, gate_weight, up_weight, down_weight, pool, pool_bias, pool_scale.reshape(1, width),
        gain_first.reshape(1, width), gain_mix.reshape(1, width), gain_second.reshape(1, width),
    )


def layer(n_grp, n, n_tp, *args):
    n_rows, width = args[0].shape
    d_loc, f_loc = args[1].shape
    pool_rows, _, pool_cols = args[4].shape
    fits = n_grp == 2 and n_tp == 4 and n % 2 == 0 and n <= 4 and n_rows % 64 == 0
    fits = fits and d_loc % 512 == 0 and f_loc % 256 == 0 and pool_rows % 32 == 0 and pool_cols % 128 == 0
    return fused_shards(n, n_tp, *args) if fits else shards(*args)


def solution(mesh):
    return jax.shard_map(
        functools.partial(layer, mesh.shape["grp"], mesh.shape["fs"], mesh.shape["tp"]),
        mesh=mesh,
        in_specs=(
            P(("grp", "fs"), None),
            P("fs", "tp"),
            P("fs", "tp"),
            P("tp", "fs"),
            P("fs", None, "tp"),
            P(),
            P(),
            P(),
            P(),
            P(),
        ),
        out_specs=P(("grp", "fs"), None),
        check_vma=False,
    )
```

profile of v0, /device:TPU:0, one launch (start us, length us, event | category | flops | bytes accessed | tf_op | source)
XLA Modules:
  0.0 192.4 jit_solution(11247294013662869065)
XLA Ops:
  0.0 1.6 copy.13
  1.6 188.1 %shard_map.100 = bf16[384,2048]{1,0:T(8,128)(2,1)} custom-call(bf16[384,2048]{1,0:T(8,128)(2,1)} %tok_ref.1, bf16[512,1280]{1,0:T(8,128)(2,1)} %gate_ref.1, bf16[512,1280]{1,0:T(8,128)(2,1)} %up_ref.1, bf16[1280,512]{1,0:T(8,128)(2,1)} %down_ref.1, bf16[4,128,128]{2,1,0:T(8,128)(2,1)} %bitcast.7, f32[4,512]{1,0:T(4,128)} %bias_ref.1, f32[1,2048]{1,0:T(1,128)} %bitcast.8, ...), custom_call_target="tpu_custom_call" | custom-call | tf_op jit(solution)/shard_map/pallas_call | solution.py:463
  189.7 2.7 %copy.15 = bf16[384,2048]{1,0:T(8,128)(2,1)} copy(bf16[384,2048]{1,0:T(8,128)(2,1)} %shard_map.100) | data formatting | bytes 3145728
where the time goes:
time: 194 us; the launch traced here: 192 us
  Pallas kernels  188 us (97%)
  local copies, waits for them, and re-layouts  4.3 us (2%)
    pallas_call x1, Pallas kernels, fused_shards(): pl.pallas_call(functools.partial(fused_kernel, (n, n_tp)), out_shape=jax....  188 us
    unnamed x2, local copies, waits for them, and re-layouts  4.3 us

commit v1 on v0

v1 whole, which is shorter than its diff:
```python
import functools

import jax
import jax.numpy as jnp
from jax import lax
from jax.experimental import pallas as pl
from jax.experimental.pallas import tpu as pltpu
from jax.sharding import PartitionSpec as P

eps = 1e-06
pool_spans = (2, 4, 8, 16)
pad_width = 8
MESH = pl.DeviceIdType.MESH


def rms_scale(values, gain_vec):
    fvalues = values.astype(jnp.float32)
    scaled = fvalues * lax.rsqrt(jnp.mean(fvalues * fvalues, axis=-1, keepdims=True) + eps)
    return (scaled * gain_vec).astype(jnp.bfloat16)


def ffn_hidden(normed, gate_full, up_full):
    gate_proj = jnp.dot(normed, gate_full, preferred_element_type=jnp.float32)
    up_proj = jnp.dot(normed, up_full, preferred_element_type=jnp.float32)
    return (jax.nn.silu(gate_proj) * up_proj).astype(jnp.bfloat16)


def pool_block(padded, offset, seq_len, pool_full, pool_bias, pool_scale):
    n_tokens = padded.shape[0] - 2 * pad_width
    group_width = pool_full.shape[0]
    position = offset + lax.iota(jnp.int32, n_tokens)
    column_pos = offset - pad_width + lax.iota(jnp.int32, padded.shape[0])
    center = padded[pad_width : pad_width + n_tokens].astype(jnp.float32)
    outputs = []
    for group_number, window_span in enumerate(pool_spans):
        low_edge = jnp.clip(position - window_span // 2, 0, seq_len)
        high_edge = jnp.clip(position - window_span // 2 + window_span, 0, seq_len)
        band_mask = (
            (column_pos[None, :] >= low_edge[:, None]) & (column_pos[None, :] < high_edge[:, None])
        ).astype(jnp.bfloat16)
        lower_col = group_number * group_width
        columns = padded[:, lower_col : lower_col + group_width]
        window_sum = jnp.dot(band_mask, columns, preferred_element_type=jnp.float32)
        window_mean = window_sum / (high_edge - low_edge).astype(jnp.float32)[:, None]
        deviation = (window_mean - center[:, lower_col : lower_col + group_width]).astype(
            jnp.bfloat16
        )
        mapped = jnp.dot(
            deviation, pool_full[:, group_number, :], preferred_element_type=jnp.float32
        )
        outputs.append(mapped + pool_bias[group_number])
    return jnp.concatenate(outputs, axis=-1) * pool_scale


def shards(
    tokens,
    gate_weight,
    up_weight,
    down_weight,
    pool_weight,
    pool_bias,
    pool_scale,
    gain_first,
    gain_mix,
    gain_second,
):
    gate_full, up_full, pool_half = (
        lax.all_gather(gate_weight, "fs", axis=0, tiled=True),
        lax.all_gather(up_weight, "fs", axis=0, tiled=True),
        lax.all_gather(pool_weight, "fs", axis=0, tiled=True),
    )
    down_full = lax.all_gather(down_weight, "fs", axis=1, tiled=True)
    pool_full = lax.all_gather(pool_half, "tp", axis=2, tiled=True)
    seq_len = tokens.shape[0]
    first_normed = rms_scale(tokens, gain_first)
    first_hidden = ffn_hidden(first_normed, gate_full, up_full)
    second_gate, second_up, second_down = (gate_full, up_full, down_full)
    first_branch = lax.psum(
        jnp.dot(first_hidden, down_full, preferred_element_type=jnp.float32).astype(jnp.bfloat16),
        "tp",
    ).astype(jnp.float32)
    after_first = (tokens.astype(jnp.float32) + 0.5 * first_branch).astype(jnp.bfloat16)
    mix_normed = rms_scale(after_first, gain_mix)
    padded = jnp.pad(mix_normed, ((pad_width, pad_width), (0, 0)))
    mixed = pool_block(padded, 0, seq_len, pool_full, pool_bias, pool_scale)
    after_mix = (after_first.astype(jnp.float32) + mixed).astype(jnp.bfloat16)
    second_normed = rms_scale(after_mix, gain_second)
    second_hidden = ffn_hidden(second_normed, second_gate, second_up)
    second_branch = lax.psum(
        jnp.dot(second_hidden, second_down, preferred_element_type=jnp.float32).astype(
            jnp.bfloat16
        ),
        "tp",
    ).astype(jnp.float32)
    return (after_mix.astype(jnp.float32) + 0.5 * second_branch).astype(jnp.bfloat16)


def fused_kernel(
    sizes, tok_ref, gate_ref, up_ref, down_ref, pool_ref, bias_ref, scale_ref, gain1_ref, gainm_ref, gain2_ref,
    out_ref,
    gu_full, down_full, pool_full, acc, normed, hidden, amix, res, guest, part0, rbuf0, xs0, xr0, xg0, lent,
    part1, rbuf1, xs1, xr1,
    zsend, zleft, zrecv, ysend, yrecv, tsend, trecv, lsem, asend, arecv, qsend, qrecv,
    csend, crecv, xsend, xrecv, gsend, grecv, fsend, frecv, osem,
):
    n, n_tp = sizes
    g, z, t = lax.axis_index("grp"), lax.axis_index("fs"), lax.axis_index("tp")
    core, side = lax.rem(t, 2), t // 2
    outer = (z == 0) | (z == n - 1)
    inner = (z > 0) & (z < n - 1)
    e = 1 - jnp.minimum(z, 1) * jnp.minimum(n - 1 - z, 1)
    pz = z + 1 - 2 * lax.rem(z, 2)
    mirror, far = n - 1 - z, n - 1 - pz
    y_peer, partner, inward = {"grp": 1 - g}, {"fs": pz}, {"fs": mirror}
    mate, x_peer = {"tp": t + 1 - 2 * core}, {"tp": lax.rem(t + 2, n_tp)}
    n_rows, width = tok_ref.shape
    d_loc, f_loc = gate_ref.shape
    groups, pool_rows, pool_cols = pool_ref.shape
    half_rows = n_rows // 2
    quarter = n_rows // n_tp
    block_cols = d_loc // 2
    n_blocks = 2 * n
    f32 = jnp.float32

    def remote(src, dst, s_sem, r_sem, dev):
        return pltpu.make_async_remote_copy(
            src_ref=src, dst_ref=dst, send_sem=s_sem, recv_sem=r_sem, device_id=dev, device_id_type=MESH
        )

    barrier = pltpu.get_barrier_semaphore()

    def greet(dev):
        pl.semaphore_signal(barrier, inc=1, device_id=dev, device_id_type=MESH)

    greet(y_peer)
    greet(partner)
    for off in range(1, n_tp):
        greet({"tp": lax.rem(t + off, n_tp)})

    @pl.when(inner)
    def _():
        greet(inward)

    pl.semaphore_wait(barrier, n_tp + 2 - e)

    counts = {"pool": 1, "gu": 8, "down": 4}
    first_key = {"pool": 0, "gu": 1, "down": 9}

    def each(name, act):
        if counts[name] == 1:
            act(0)
        else:
            pl.loop(0, counts[name])(act)

    def key(name, c):
        return first_key[name] + c

    def region(name, s, half, c):
        if name == "down":
            size = f_loc // 4
            return down_full.at[s, half, pl.ds(pl.multiple_of(c * size, 16), size), :]
        if name == "pool":
            size = pool_rows // 2
            rows = pl.ds(pl.multiple_of(s * pool_rows + half * size, 16), size)
            return pool_full.at[:, rows, pl.ds(pl.multiple_of(t * pool_cols, 128), pool_cols)]
        size = d_loc // 8
        rows = pl.ds(pl.multiple_of(s * d_loc + half * (d_loc // 2) + lax.rem(c, 4) * size, 16), size)
        return gu_full.at[c // 4, rows, :]

    def source(name, half, c):
        if name == "down":
            size = f_loc // 4
            cols = pl.ds(pl.multiple_of(half * block_cols, 128), block_cols)
            return down_ref.at[pl.ds(pl.multiple_of(c * size, 16), size), cols]
        if name == "pool":
            size = pool_rows // 2
            return pool_ref.at[:, pl.ds(pl.multiple_of(half * size, 16), size), :]
        size = d_loc // 8
        rows = pl.ds(pl.multiple_of(half * (d_loc // 2) + c * size, 16), size)
        return {"gate": gate_ref, "up": up_ref}[name].at[rows, :]

    def own_copy(name, c, half, s_sem, r_sem, dev):
        base = {"gate": 0, "up": 4}.get(name)
        k = key("gu", base + c) if base is not None else key(name, c)
        where = region("gu", z, half, base + c) if base is not None else region(name, z, half, c)
        return remote(source(name, half, c), where, s_sem.at[k], r_sem.at[z, k], dev)

    def own_partner(name, c):
        return own_copy(name, c, g, zsend.at[z], zrecv, partner)

    def own_inward(name, c):
        return own_copy(name, c, g, zleft, zrecv, inward)

    def own_direct(name, c):
        return own_copy(name, c, 1 - g, ysend.at[z], yrecv, partner)

    def passing(name, s, c, dev):
        there = region(name, s, g, c)
        return remote(there, there, zsend.at[s, key(name, c)], zrecv.at[s, key(name, c)], dev)

    def share(name, s, half, c):
        there = region(name, s, half, c)
        return remote(there, there, ysend.at[s, key(name, c)], yrecv.at[s, key(name, c)], y_peer)

    def settle(name, s, low=0, high=None):
        if counts[name] == 1:
            share(name, s, 1 - g, 0).wait_recv()
        else:
            pl.loop(low, counts[name] if high is None else high)(lambda c: share(name, s, 1 - g, c).wait_recv())

    def quarter_rows(tt):
        return pl.ds(pl.multiple_of((lax.rem(tt, 2) * (n_tp // 2) + tt // 2) * quarter, 16), quarter)

    def start_each(names, make):
        for name in names:
            pl.loop(0, 1 if name == "pool" else 4)(lambda c: make(name, c).start())

    tok_copy = remote(
        tok_ref.at[quarter_rows(t), :], guest.at[quarter_rows(t), :], asend.at[0], arecv.at[0], partner
    )

    @pl.when(outer)
    def _():
        tok_copy.start()
        start_each(("pool", "gate", "up"), own_partner)
        start_each(("pool", "gate", "up"), own_direct)
        start_each(("down",), own_partner)
        pl.loop(0, 2)(lambda c: own_direct("down", c).start())

    @pl.when(inner)
    def _():
        for name in ("pool", "gate", "up"):

            @pl.loop(0, 1 if name == "pool" else 4)
            def _(c):
                own_inward(name, c).start()
                own_partner(name, c).start()

    own_rows = pl.ds(pl.multiple_of(z * d_loc, 128), d_loc)
    own_pool = pool_full.at[
        :, pl.ds(pl.multiple_of(z * pool_rows, 16), pool_rows), pl.ds(pl.multiple_of(t * pool_cols, 128), pool_cols)
    ]
    local = [
        pltpu.make_async_copy(pool_ref, own_pool, lsem.at[0]),
        pltpu.make_async_copy(gate_ref, gu_full.at[0, own_rows, :], lsem.at[1]),
        pltpu.make_async_copy(up_ref, gu_full.at[1, own_rows, :], lsem.at[2]),
        pltpu.make_async_copy(down_ref.at[:, pl.ds(0, block_cols)], down_full.at[z, 0], lsem.at[3]),
        pltpu.make_async_copy(down_ref.at[:, pl.ds(block_cols, block_cols)], down_full.at[z, 1], lsem.at[4]),
    ]
    for copy in local:
        copy.start()

    def norm_rows(src, gain, base=0):
        @pl.loop(0, n_rows // 32)
        def _(r):
            values = src[pl.ds(pl.multiple_of(r * 32, 32), 32), :].astype(f32)
            scaled = values * lax.rsqrt(jnp.mean(values * values, axis=-1, keepdims=True) + eps)
            normed[pl.ds(pl.multiple_of(base + r * 32, 32), 32), :] = (scaled * gain[...]).astype(jnp.bfloat16)

    tile = 256

    def add_shard(w, s, first=False):
        k_cols = pl.ds(pl.multiple_of(s * d_loc, 128), d_loc)

        @pl.loop(0, f_loc // tile)
        def _(i):
            cols = pl.ds(pl.multiple_of(i * tile, tile), tile)
            product = jnp.dot(normed[:, k_cols], gu_full[w, k_cols, cols], preferred_element_type=f32)
            acc[w, :, cols] = product if first else acc[w, :, cols] + product

    def pool_copy(off, s, sender):
        cols = pl.ds(pl.multiple_of(sender * pool_cols, 128), pool_cols)
        there = pool_full.at[:, pl.ds(pl.multiple_of(s * pool_rows, 16), pool_rows), cols]
        return remote(there, there, tsend.at[off - 1, s], trecv.at[off - 1, s], {"tp": lax.rem(t + off, n_tp)})

    def spread_pool(s):
        for off in range(1, n_tp):
            pool_copy(off, s, t).start()

    def activate(gate_proj, up_proj):
        return (gate_proj / (1.0 + jnp.exp(-gate_proj)) * up_proj).astype(jnp.bfloat16)

    def guest_copy(off, sender):
        there = guest.at[quarter_rows(sender), :]
        return remote(there, there, qsend.at[off - 1, 0], qrecv.at[off - 1, 0], {"tp": lax.rem(t + off, n_tp)})

    def columns(place):
        s, half = place
        return pl.ds(pl.multiple_of(s * d_loc + half * block_cols, 128), block_cols)

    def first_place(j, at):
        here = [at, n - 1 - at, at + 1 - 2 * lax.rem(at, 2)]
        here.append(n - 1 - here[2])
        shard, half = ((0, 0), (0, 1), (1, 0), (1, 1), (2, 0), (3, 0), (2, 1), (3, 1))[j]
        return here[shard], g if half == 0 else 1 - g

    def second_place(j):
        here = [z, e * pz + (1 - e) * mirror, e * far + (1 - e) * pz, e * mirror + (1 - e) * far]
        return here[j // 2], g if j % 2 == 0 else 1 - g

    mine = pl.ds(pl.multiple_of(core * half_rows, 16), half_rows)
    other = pl.ds(pl.multiple_of((1 - core) * half_rows, 16), half_rows)

    def final_copy(phase, j, place, rows):
        there = res.at[phase, rows, columns(place)]
        return remote(there, there, fsend.at[phase, j], frecv.at[phase, j], mate)

    def pair_first(j):
        return remote(part0.at[j, 1 - core], rbuf0.at[j], csend.at[0, j], crecv.at[0, j], mate)

    def x_first(j):
        return remote(xs0.at[j, 0], xr0.at[j], xsend.at[0, j], xrecv.at[0, j], x_peer)

    kept = pl.ds(pl.multiple_of(side * quarter, 16), quarter)
    given = pl.ds(pl.multiple_of((1 - side) * quarter, 16), quarter)

    def x_guest(j):
        return remote(xs0.at[j, 1, given, :], xg0.at[j], gsend.at[j], grecv.at[j], x_peer)

    def lend_copy(j, at):
        cols = columns(first_place(j, at))
        return remote(lent.at[j], res.at[0, quarter_rows(t), cols], asend.at[1 + j], arecv.at[1 + j], partner)

    def lent_copy(j, off, sender):
        there = res.at[0, quarter_rows(sender), columns(first_place(j, pz))]
        return remote(
            there, there, qsend.at[off - 1, 1 + j], qrecv.at[off - 1, 1 + j], {"tp": lax.rem(t + off, n_tp)}
        )

    def from_mirror(name, c):
        passing(name, mirror, c, partner).wait_recv()
        passing(name, mirror, c, partner).start()
        share(name, mirror, g, c).start()

    def from_far(name, c):
        passing(name, far, c, partner).wait_recv()
        passing(name, far, c, partner).start()
        share(name, far, g, c).start()

    def from_partner(name, c):
        passing(name, pz, c, inward).wait_recv()
        passing(name, pz, c, inward).start()

    def down_mirror(c):
        passing("down", mirror, c, partner).wait_recv()
        share("down", mirror, g, c).start()

    def down_far(c):
        passing("down", far, c, partner).wait_recv()
        share("down", far, g, c).start()

    def down_partner(c, shared):
        from_partner("down", c)
        if shared:
            share("down", pz, g, c).start()

    def first_ffn():
        for copy in local:
            copy.wait()
        spread_pool(z)
        norm_rows(tok_ref, gain1_ref)
        tok_copy.wait_recv()
        for off in range(1, n_tp):
            guest_copy(off, t).start()
        from_mirror("pool", 0)
        from_mirror("gu", 0)
        from_mirror("gu", 1)
        from_partner("pool", 0)

        @pl.loop(0, 4)
        def _(m):
            from_mirror("gu", m + 2)
            from_partner("gu", m)

        for off in range(1, n_tp):
            guest_copy(off, lax.rem(t - off + n_tp, n_tp)).wait_recv()
        norm_rows(guest, gain1_ref, n_rows)
        from_mirror("gu", 6)
        from_partner("gu", 4)
        add_shard(0, z, True)
        from_mirror("gu", 7)
        from_partner("gu", 5)
        add_shard(1, z, True)
        settle("pool", mirror)
        spread_pool(mirror)
        from_far("pool", 0)
        from_far("gu", 0)
        from_partner("gu", 6)
        settle("gu", mirror, 0, 4)
        add_shard(0, mirror)
        from_far("gu", 1)
        from_partner("gu", 7)
        pl.loop(0, 4)(lambda c: own_inward("down", c).start())
        settle("gu", mirror, 4, 8)
        add_shard(1, mirror)
        pl.loop(2, 5)(lambda m: from_far("gu", m))
        settle("pool", far)
        spread_pool(far)
        settle("pool", pz)
        spread_pool(pz)
        settle("gu", far, 0, 4)
        add_shard(0, far)
        from_far("gu", 5)
        settle("gu", pz, 0, 4)
        add_shard(0, pz)
        pl.loop(6, 8)(lambda m: from_far("gu", m))
        settle("gu", far, 4, 8)
        add_shard(1, far)
        down_mirror(0)
        down_mirror(1)
        settle("gu", pz, 4, 8)
        add_shard(1, pz)
        down_mirror(2)

        @pl.loop(0, f_loc // tile)
        def _(i):
            cols = pl.ds(pl.multiple_of(i * tile, tile), tile)

            @pl.loop(0, 2 * n_rows // 128)
            def _(r):
                rows = pl.ds(pl.multiple_of(r * 128, 128), 128)
                hidden[rows, cols] = activate(acc[0, rows, cols], acc[1, rows, cols])

        def multiply(j):
            s, half = first_place(j, z)
            product = jnp.dot(hidden[...], down_full[s, half], preferred_element_type=f32).astype(jnp.bfloat16)
            for seq in range(2):
                for part in range(2):
                    row = seq * n_rows + part * half_rows
                    part0[j, part, seq] = product[row : row + half_rows]
            pair_first(j).start()

        def add_pair(j):
            pair_first(j).wait_recv()
            xs0[j] = (part0[j, core].astype(f32) + rbuf0[j].astype(f32)).astype(jnp.bfloat16)
            x_guest(j).start()
            x_first(j).start()

        def finish(j):
            place = first_place(j, z)
            cols = columns(place)
            x_guest(j).wait_recv()
            total = xs0[j, 1, kept, :].astype(f32) + xg0[j].astype(f32)
            lent[j] = (guest[quarter_rows(t), cols].astype(f32) + 0.5 * total).astype(jnp.bfloat16)
            lend_copy(j, z).start()
            x_first(j).wait_recv()
            total = xs0[j, 0].astype(f32) + xr0[j].astype(f32)
            res[0, mine, cols] = (tok_ref[mine, cols].astype(f32) + 0.5 * total).astype(jnp.bfloat16)
            final_copy(0, j, place, mine).start()

        down_partner(0, False)
        down_mirror(3)
        for j in range(n_blocks):
            if j == 2:
                down_partner(1, False)
                down_far(0)
                settle("down", mirror)
            if j == 4:
                down_partner(2, True)
                down_far(1)
                down_partner(3, True)
                down_far(2)
            if j == 5:
                down_far(3)
            if j == 6:
                settle("down", pz)
            if j == 7:
                settle("down", far)
            multiply(j)
            if j >= 1:
                add_pair(j - 1)
            if j >= 3:
                finish(j - 3)
            if j == 5:
                own_partner("down", 0).start()
            if j == 7:
                own_partner("down", 1).start()
        add_pair(n_blocks - 1)
        for j in range(n_blocks - 3, n_blocks):
            finish(j)
        own_partner("down", 2).start()
        own_partner("down", 3).start()
        pl.loop(0, 4)(lambda c: passing("down", mirror, c, partner).start())
        pl.loop(0, 4)(lambda c: passing("down", far, c, partner).start())
        for j in range(n_blocks):
            final_copy(0, j, first_place(j, z), other).wait_recv()

    def take(name, s, c):
        passing(name, s, c, partner).wait_recv()
        share(name, s, g, c).start()

    def collect():
        for copy in local:
            copy.wait()
        spread_pool(z)
        for s in (pz, far, mirror):
            take("pool", s, 0)
            pl.loop(0, 8)(lambda m: take("gu", s, m))
            settle("pool", s)
            spread_pool(s)

        def hand_out(j):
            lend_copy(j, pz).wait_recv()
            for off in range(1, n_tp):
                lent_copy(j, off, t).start()

        for j in range(n_blocks):
            hand_out(j)
            if j == 2:
                take("down", pz, 0)
            if j == 4:
                take("down", pz, 1)
        for s in (pz, far, mirror):
            settle("gu", s)
        for j in range(n_blocks):
            for off in range(1, n_tp):
                lent_copy(j, off, lax.rem(t - off + n_tp, n_tp)).wait_recv()

    pl.when(inner)(first_ffn)
    pl.when(outer)(collect)

    def when_outer(act):
        pl.when(outer)(act)

    norm_rows(res.at[0], gainm_ref)
    for off in range(1, n_tp):
        for s in range(n):
            pool_copy(off, s, lax.rem(t - off + n_tp, n_tp)).wait_recv()
    group_width = width // groups
    row_id = lax.broadcasted_iota(jnp.int32, (n_rows, n_rows), 0)
    col_id = lax.broadcasted_iota(jnp.int32, (n_rows, n_rows), 1)
    position = lax.broadcasted_iota(jnp.int32, (n_rows, 1), 0)
    own_seq = pl.ds(0, n_rows)
    for k, span in enumerate(pool_spans):
        low = row_id - span // 2
        band = jnp.where((col_id >= low) & (col_id < low + span), 1.0, 0.0).astype(jnp.bfloat16)
        first = jnp.maximum(position - span // 2, 0)
        last = jnp.minimum(position - span // 2 + span, n_rows)
        inverse = 1.0 / (last - first).astype(f32)
        cols = pl.ds(k * group_width, group_width)
        mean = jnp.dot(band, normed[own_seq, cols], preferred_element_type=f32) * inverse
        deviation = (mean - normed[own_seq, cols].astype(f32)).astype(jnp.bfloat16)
        mapped = jnp.dot(deviation, pool_full[k], preferred_element_type=f32) + bias_ref[pl.ds(k, 1), :]
        amix[:, cols] = (res[0, :, cols].astype(f32) + mapped * scale_ref[:, cols]).astype(jnp.bfloat16)
        if k % 2 == 1:
            when_outer(lambda: take("down", pz, 2 + k // 2))

    norm_rows(amix, gain2_ref)

    @pl.loop(0, f_loc // tile)
    def _(i):
        cols = pl.ds(pl.multiple_of(i * tile, tile), tile)
        gate_proj = jnp.dot(normed[own_seq, :], gu_full[0, :, cols], preferred_element_type=f32)
        up_proj = jnp.dot(normed[own_seq, :], gu_full[1, :, cols], preferred_element_type=f32)
        hidden[own_seq, cols] = activate(gate_proj, up_proj)

        @pl.when(outer & (i < 4))
        def _():
            take("down", far, i)

    def pair_copy(j):
        return remote(part1.at[j, other, :], rbuf1.at[j], csend.at[1, j], crecv.at[1, j], mate)

    def x_copy(j):
        return remote(xs1.at[j], xr1.at[j], xsend.at[1, j], xrecv.at[1, j], x_peer)

    def out_copy(j):
        cols = columns(second_place(j))
        return pltpu.make_async_copy(res.at[1, :, cols], out_ref.at[:, cols], osem.at[j])

    def multiply(j):
        s, half = second_place(j)
        part1[j] = jnp.dot(hidden[own_seq, :], down_full[s, half], preferred_element_type=f32).astype(jnp.bfloat16)
        pair_copy(j).start()

    def add_pair(j):
        pair_copy(j).wait_recv()
        xs1[j] = (part1[j, mine, :].astype(f32) + rbuf1[j].astype(f32)).astype(jnp.bfloat16)
        x_copy(j).start()

    def finish(j):
        x_copy(j).wait_recv()
        place = second_place(j)
        cols = columns(place)
        total = xs1[j].astype(f32) + xr1[j].astype(f32)
        res[1, mine, cols] = (amix[mine, cols].astype(f32) + 0.5 * total).astype(jnp.bfloat16)
        final_copy(1, j, place, mine).start()

    def emit(j):
        final_copy(1, j, second_place(j), other).wait_recv()
        out_copy(j).start()

    for j in range(n_blocks):
        if j == 3:
            when_outer(lambda: settle("down", pz))
        if j == 5:
            when_outer(lambda: settle("down", far))
        if 3 <= j < 7:
            when_outer(lambda: take("down", mirror, j - 3))
        if j == 7:
            when_outer(lambda: settle("down", mirror))
        multiply(j)
        if j >= 1:
            add_pair(j - 1)
        if j >= 3:
            finish(j - 3)
        if j >= 5:
            emit(j - 5)
    add_pair(n_blocks - 1)
    for j in range(n_blocks - 3, n_blocks):
        finish(j)
    for j in range(n_blocks - 5, n_blocks):
        emit(j)

    @pl.loop(0, n)
    def _(s):
        for off in range(1, n_tp):
            pool_copy(off, s, t).wait_send()

    for name in ("pool", "gate", "up", "down"):
        pl.loop(0, 1 if name == "pool" else 4)(lambda c: own_partner(name, c).wait_send())

    @pl.when(outer)
    def _():
        tok_copy.wait_send()
        for name in ("pool", "gate", "up", "down"):
            direct = {"pool": 1, "down": 2}.get(name, 4)
            pl.loop(0, direct)(lambda c: own_direct(name, c).wait_send())
        for s in (pz, far, mirror):
            for name in ("pool", "gu", "down"):
                each(name, lambda c: share(name, s, g, c).wait_send())
        for j in range(n_blocks):
            for off in range(1, n_tp):
                lent_copy(j, off, t).wait_send()

    @pl.when(inner)
    def _():
        for off in range(1, n_tp):
            guest_copy(off, t).wait_send()
        for name in ("pool", "gate", "up", "down"):
            pl.loop(0, 1 if name == "pool" else 4)(lambda c: own_inward(name, c).wait_send())
        for name in ("pool", "gu", "down"):
            each(name, lambda c: passing(name, pz, c, inward).wait_send())
            for s in (mirror, far):

                def sent(c):
                    passing(name, s, c, partner).wait_send()
                    share(name, s, g, c).wait_send()

                each(name, sent)
        pl.loop(2, 4)(lambda c: share("down", pz, g, c).wait_send())
        for j in range(n_blocks):
            pair_first(j).wait_send()
            x_first(j).wait_send()
            x_guest(j).wait_send()
            lend_copy(j, z).wait_send()
            final_copy(0, j, first_place(j, z), mine).wait_send()

    for j in range(n_blocks):
        pair_copy(j).wait_send()
        x_copy(j).wait_send()
        final_copy(1, j, second_place(j), mine).wait_send()
        out_copy(j).wait()


def fused_shards(
    n, n_tp, tokens, gate_weight, up_weight, down_weight, pool_weight, pool_bias, pool_scale,
    gain_first, gain_mix, gain_second,
):
    n_rows, width = tokens.shape
    d_loc, f_loc = gate_weight.shape
    groups = pool_weight.shape[1]
    pool = jnp.swapaxes(pool_weight, 0, 1)
    bf16, dma, vmem = jnp.bfloat16, pltpu.SemaphoreType.DMA, pltpu.VMEM
    in_vmem, anywhere = pl.BlockSpec(memory_space=pltpu.VMEM), pl.BlockSpec(memory_space=pl.ANY)
    half, quarter, block, blocks = n_rows // 2, n_rows // n_tp, d_loc // 2, 2 * n
    return pl.pallas_call(
        functools.partial(fused_kernel, (n, n_tp)),
        out_shape=jax.ShapeDtypeStruct((n_rows, width), bf16),
        in_specs=[in_vmem] + [anywhere] * 4 + [in_vmem] * 5,
        out_specs=anywhere,
        scratch_shapes=[
            vmem((2, n * d_loc, f_loc), bf16),
            vmem((n, 2, f_loc, block), bf16),
            vmem((groups, n * pool.shape[1], n_tp * pool.shape[2]), bf16),
            vmem((2, 2 * n_rows, f_loc), jnp.float32),
            vmem((2 * n_rows, width), bf16),
            vmem((2 * n_rows, f_loc), bf16),
            vmem((n_rows, width), bf16),
            vmem((2, n_rows, width), bf16),
            vmem((n_rows, width), bf16),
            vmem((blocks, 2, 2, half, block), bf16),
            vmem((blocks, 2, half, block), bf16),
            vmem((blocks, 2, half, block), bf16),
            vmem((blocks, half, block), bf16),
            vmem((blocks, quarter, block), bf16),
            vmem((blocks, quarter, block), bf16),
            vmem((blocks, n_rows, block), bf16),
            vmem((blocks, half, block), bf16),
            vmem((blocks, half, block), bf16),
            vmem((blocks, half, block), bf16),
            dma((n, 13)), dma((13,)), dma((n, 13)), dma((n, 13)), dma((n, 13)),
            dma((n_tp - 1, n)), dma((n_tp - 1, n)), dma((5,)),
            dma((1 + blocks,)), dma((1 + blocks,)), dma((n_tp - 1, 1 + blocks)), dma((n_tp - 1, 1 + blocks)),
            dma((2, blocks)), dma((2, blocks)), dma((2, blocks)), dma((2, blocks)), dma((blocks,)), dma((blocks,)),
            dma((2, blocks)), dma((2, blocks)), dma((blocks,)),
        ],
        compiler_params=pltpu.CompilerParams(
            collective_id=0, has_side_effects=True, vmem_limit_bytes=60 * 1024 * 1024
        ),
    )(
        tokens, gate_weight, up_weight, down_weight, pool, pool_bias, pool_scale.reshape(1, width),
        gain_first.reshape(1, width), gain_mix.reshape(1, width), gain_second.reshape(1, width),
    )


def layer(n_grp, n, n_tp, *args):
    n_rows, width = args[0].shape
    d_loc, f_loc = args[1].shape
    pool_rows, _, pool_cols = args[4].shape
    fits = n_grp == 2 and n_tp == 4 and n == 4 and n_rows % 64 == 0
    fits = fits and d_loc % 512 == 0 and f_loc % 256 == 0 and pool_rows % 32 == 0 and pool_cols % 128 == 0
    return fused_shards(n, n_tp, *args) if fits else shards(*args)


def solution(mesh):
    return jax.shard_map(
        functools.partial(layer, mesh.shape["grp"], mesh.shape["fs"], mesh.shape["tp"]),
        mesh=mesh,
        in_specs=(
            P(("grp", "fs"), None),
            P("fs", "tp"),
            P("fs", "tp"),
            P("tp", "fs"),
            P("fs", None, "tp"),
            P(),
            P(),
            P(),
            P(),
            P(),
        ),
        out_specs=P(("grp", "fs"), None),
        check_vma=False,
    )
```

time: 194 us -> 186 us (0.959)
  Pallas kernels: 188 us -> 181 us
    pallas_call x1, Pallas kernels: 188 us -> 181 us  [fused_shards(): pl.pallas_call(functools.partial(fused_kernel, (n, n_tp)), out_shape=jax....]
where the time goes in v1:
time: 186 us; the launch traced here: 185 us
  Pallas kernels  181 us (97%)
  local copies, waits for them, and re-layouts  4.3 us (2%)
    pallas_call x1, Pallas kernels, fused_shards(): pl.pallas_call(functools.partial(fused_kernel, (n, n_tp)), out_shape=jax....  181 us
    unnamed x2, local copies, waits for them, and re-layouts  4.3 us

profile of v1, /device:TPU:0, one launch (start us, length us, event | category | flops | bytes accessed | tf_op | source)
XLA Modules:
  0.0 185.1 jit_solution(2058261797793339621)
XLA Ops:
  0.0 1.6 copy.13
  1.6 180.8 %shard_map.100 = bf16[384,2048]{1,0:T(8,128)(2,1)} custom-call(bf16[384,2048]{1,0:T(8,128)(2,1)} %tok_ref.1, bf16[512,1280]{1,0:T(8,128)(2,1)} %gate_ref.1, bf16[512,1280]{1,0:T(8,128)(2,1)} %up_ref.1, bf16[1280,512]{1,0:T(8,128)(2,1)} %down_ref.1, bf16[4,128,128]{2,1,0:T(8,128)(2,1)} %bitcast.7, f32[4,512]{1,0:T(4,128)} %bias_ref.1, f32[1,2048]{1,0:T(1,128)} %bitcast.8, ...), custom_call_target="tpu_custom_call" | custom-call | tf_op jit(solution)/shard_map/pallas_call | solution.py:677
  182.4 2.7 %copy.15 = bf16[384,2048]{1,0:T(8,128)(2,1)} copy(bf16[384,2048]{1,0:T(8,128)(2,1)} %shard_map.100) | data formatting | bytes 3145728

commit v2 on v1

--- a/solution.py
+++ b/solution.py
@@ -143,7 +143,7 @@
 
     pl.semaphore_wait(barrier, n_tp + 2 - e)
 
-    counts = {"pool": 1, "gu": 8, "down": 4}
+    counts = {"pool": 1, "gu": 8, "down": 8}
     first_key = {"pool": 0, "gu": 1, "down": 9}
 
     def each(name, act):
@@ -152,12 +152,20 @@
         else:
             pl.loop(0, counts[name])(act)
 
+    kind = {"pool": 0, "gu": 1, "down": 2}
+
     def key(name, c):
         return first_key[name] + c
 
+    def slot(s, at):
+        return lax.rem(s - at + n, n) - 1
+
+    def bulk(name, c):
+        return 0 if name == "pool" else 3 if name == "down" else 1 + c // 4
+
     def region(name, s, half, c):
         if name == "down":
-            size = f_loc // 4
+            size = f_loc // 8
             return down_full.at[s, half, pl.ds(pl.multiple_of(c * size, 16), size), :]
         if name == "pool":
             size = pool_rows // 2
@@ -167,9 +175,17 @@
         rows = pl.ds(pl.multiple_of(s * d_loc + half * (d_loc // 2) + lax.rem(c, 4) * size, 16), size)
         return gu_full.at[c // 4, rows, :]
 
+    def whole(name, s, half):
+        if name == "down":
+            return down_full.at[s, half]
+        if name == "pool":
+            return region(name, s, half, 0)
+        rows = pl.ds(pl.multiple_of(s * d_loc + half * (d_loc // 2), 16), d_loc // 2)
+        return gu_full.at[:, rows, :] if name == "gu" else gu_full.at[0 if name == "gate" else 1, rows, :]
+
     def source(name, half, c):
         if name == "down":
-            size = f_loc // 4
+            size = f_loc // 8
             cols = pl.ds(pl.multiple_of(half * block_cols, 128), block_cols)
             return down_ref.at[pl.ds(pl.multiple_of(c * size, 16), size), cols]
         if name == "pool":
@@ -181,39 +197,51 @@
 
     def own_copy(name, c, half, s_sem, r_sem, dev):
         base = {"gate": 0, "up": 4}.get(name)
-        k = key("gu", base + c) if base is not None else key(name, c)
-        where = region("gu", z, half, base + c) if base is not None else region(name, z, half, c)
-        return remote(source(name, half, c), where, s_sem.at[k], r_sem.at[z, k], dev)
+        name_of, at = ("gu", base + c) if base is not None else (name, c)
+        where = region(name_of, z, half, at)
+        return remote(source(name, half, c), where, s_sem.at[kind[name_of]], r_sem(name_of, at), dev)
 
     def own_partner(name, c):
-        return own_copy(name, c, g, zsend.at[z], zrecv, partner)
+        return own_copy(name, c, g, zsend.at[z], lambda nm, at: zrecv.at[slot(z, pz), key(nm, at)], partner)
 
     def own_inward(name, c):
-        return own_copy(name, c, g, zleft, zrecv, inward)
+        return own_copy(name, c, g, zleft, lambda nm, at: zrecv.at[slot(z, mirror), key(nm, at)], inward)
 
     def own_direct(name, c):
-        return own_copy(name, c, 1 - g, ysend.at[z], yrecv, partner)
+        return own_copy(name, c, 1 - g, ysend.at[z], lambda nm, at: yrecv.at[slot(z, pz), bulk(nm, at)], partner)
 
     def passing(name, s, c, dev):
         there = region(name, s, g, c)
-        return remote(there, there, zsend.at[s, key(name, c)], zrecv.at[s, key(name, c)], dev)
-
-    def share(name, s, half, c):
-        there = region(name, s, half, c)
-        return remote(there, there, ysend.at[s, key(name, c)], yrecv.at[s, key(name, c)], y_peer)
-
-    def settle(name, s, low=0, high=None):
-        if counts[name] == 1:
-            share(name, s, 1 - g, 0).wait_recv()
-        else:
-            pl.loop(low, counts[name] if high is None else high)(lambda c: share(name, s, 1 - g, c).wait_recv())
+        to = pz if dev is partner else mirror
+        return remote(there, there, zsend.at[s, kind[name]], zrecv.at[slot(s, to), key(name, c)], dev)
+
+    def arrival(name, s, c):
+        there = region(name, s, g, c)
+        return remote(there, there, zsend.at[s, kind[name]], zrecv.at[slot(s, z), key(name, c)], partner)
+
+    def share(name, s, c):
+        there = region(name, s, g, c)
+        return remote(there, there, ysend.at[s, kind[name]], yrecv.at[slot(s, z), bulk(name, c)], y_peer)
+
+    def settle(name, s):
+        there = whole(name, s, 1 - g)
+        where = {"pool": 0, "gate": 1, "up": 2, "down": 3}[name]
+        remote(there, there, ysend.at[s, 0], yrecv.at[slot(s, z), where], y_peer).wait_recv()
+
+    def sent(name, s, half, sems, dev):
+        there = whole(name, s, half)
+        return remote(there, there, sems.at[kind[name]], yrecv.at[0, 0], dev)
+
+    kinds = ("pool", "gu", "down")
 
     def quarter_rows(tt):
         return pl.ds(pl.multiple_of((lax.rem(tt, 2) * (n_tp // 2) + tt // 2) * quarter, 16), quarter)
 
+    own_counts = {"pool": 1, "gate": 4, "up": 4, "down": 8}
+
     def start_each(names, make):
         for name in names:
-            pl.loop(0, 1 if name == "pool" else 4)(lambda c: make(name, c).start())
+            pl.loop(0, own_counts[name])(lambda c: make(name, c).start())
 
     tok_copy = remote(
         tok_ref.at[quarter_rows(t), :], guest.at[quarter_rows(t), :], asend.at[0], arecv.at[0], partner
@@ -225,13 +253,13 @@
         start_each(("pool", "gate", "up"), own_partner)
         start_each(("pool", "gate", "up"), own_direct)
         start_each(("down",), own_partner)
-        pl.loop(0, 2)(lambda c: own_direct("down", c).start())
+        start_each(("down",), own_direct)
 
     @pl.when(inner)
     def _():
         for name in ("pool", "gate", "up"):
 
-            @pl.loop(0, 1 if name == "pool" else 4)
+            @pl.loop(0, own_counts[name])
             def _(c):
                 own_inward(name, c).start()
                 own_partner(name, c).start()
@@ -271,7 +299,11 @@
     def pool_copy(off, s, sender):
         cols = pl.ds(pl.multiple_of(sender * pool_cols, 128), pool_cols)
         there = pool_full.at[:, pl.ds(pl.multiple_of(s * pool_rows, 16), pool_rows), cols]
-        return remote(there, there, tsend.at[off - 1, s], trecv.at[off - 1, s], {"tp": lax.rem(t + off, n_tp)})
+        return remote(there, there, tsend.at[off - 1], trecv.at[off - 1], {"tp": lax.rem(t + off, n_tp)})
+
+    def pool_all(off, sender):
+        there = pool_full.at[:, :, pl.ds(pl.multiple_of(sender * pool_cols, 128), pool_cols)]
+        return remote(there, there, tsend.at[off - 1], trecv.at[off - 1], {"tp": lax.rem(t + off, n_tp)})
 
     def spread_pool(s):
         for off in range(1, n_tp):
@@ -282,7 +314,7 @@
 
     def guest_copy(off, sender):
         there = guest.at[quarter_rows(sender), :]
-        return remote(there, there, qsend.at[off - 1, 0], qrecv.at[off - 1, 0], {"tp": lax.rem(t + off, n_tp)})
+        return remote(there, there, qsend.at[off - 1], qrecv.at[off - 1], {"tp": lax.rem(t + off, n_tp)})
 
     def columns(place):
         s, half = place
@@ -303,56 +335,75 @@
 
     def final_copy(phase, j, place, rows):
         there = res.at[phase, rows, columns(place)]
-        return remote(there, there, fsend.at[phase, j], frecv.at[phase, j], mate)
+        return remote(there, there, fsend.at[phase], frecv.at[phase * (1 + j)], mate)
+
+    def final_all(phase, rows):
+        there = res.at[phase, rows, :]
+        return remote(there, there, fsend.at[phase], frecv.at[0], mate)
 
     def pair_first(j):
-        return remote(part0.at[j, 1 - core], rbuf0.at[j], csend.at[0, j], crecv.at[0, j], mate)
+        return remote(part0.at[j, 1 - core], rbuf0.at[j], csend.at[0], crecv.at[0, j], mate)
 
     def x_first(j):
-        return remote(xs0.at[j, 0], xr0.at[j], xsend.at[0, j], xrecv.at[0, j], x_peer)
+        return remote(xs0.at[j, 0], xr0.at[j], xsend.at[0], xrecv.at[0, j], x_peer)
 
     kept = pl.ds(pl.multiple_of(side * quarter, 16), quarter)
     given = pl.ds(pl.multiple_of((1 - side) * quarter, 16), quarter)
 
     def x_guest(j):
-        return remote(xs0.at[j, 1, given, :], xg0.at[j], gsend.at[j], grecv.at[j], x_peer)
+        return remote(xs0.at[j, 1, given, :], xg0.at[j], gsend.at[0], grecv.at[j], x_peer)
 
     def lend_copy(j, at):
         cols = columns(first_place(j, at))
-        return remote(lent.at[j], res.at[0, quarter_rows(t), cols], asend.at[1 + j], arecv.at[1 + j], partner)
-
-    def lent_copy(j, off, sender):
-        there = res.at[0, quarter_rows(sender), columns(first_place(j, pz))]
+        return remote(lent.at[j], res.at[0, quarter_rows(t), cols], asend.at[1], arecv.at[1 + j], partner)
+
+    def lent_copy(j, lane):
+        owner = (t, t, lax.rem(t + 2, n_tp))[lane]
+        there = res.at[0, quarter_rows(owner), columns(first_place(j, pz))]
         return remote(
-            there, there, qsend.at[off - 1, 1 + j], qrecv.at[off - 1, 1 + j], {"tp": lax.rem(t + off, n_tp)}
+            there, there, qsend.at[3 + lane], qrecv.at[3 + j if lane == 1 else 11 + lane // 2], x_peer if lane == 1 else mate
         )
 
+    def lent_all(lane, owner):
+        there = res.at[0, quarter_rows(owner), :]
+        return remote(there, there, qsend.at[3 + lane], qrecv.at[11 + lane // 2], mate)
+
+    def lent_arrival(j):
+        lane = 1
+        owner = lax.rem(t + 2, n_tp)
+        there = res.at[0, quarter_rows(owner), columns(first_place(j, pz))]
+        return remote(
+            there, there, qsend.at[3 + lane], qrecv.at[3 + j if lane == 1 else 11 + lane // 2], x_peer if lane == 1 else mate
+        )
+
     def from_mirror(name, c):
-        passing(name, mirror, c, partner).wait_recv()
+        arrival(name, mirror, c).wait_recv()
         passing(name, mirror, c, partner).start()
-        share(name, mirror, g, c).start()
+        share(name, mirror, c).start()
 
     def from_far(name, c):
-        passing(name, far, c, partner).wait_recv()
+        arrival(name, far, c).wait_recv()
         passing(name, far, c, partner).start()
-        share(name, far, g, c).start()
+        share(name, far, c).start()
 
     def from_partner(name, c):
-        passing(name, pz, c, inward).wait_recv()
+        arrival(name, pz, c).wait_recv()
         passing(name, pz, c, inward).start()
 
+    def keep_down(s, low):
+        for c in range(low, low + 2):
+            arrival("down", s, c).wait_recv()
+            share("down", s, c).start()
+
     def down_mirror(c):
-        passing("down", mirror, c, partner).wait_recv()
-        share("down", mirror, g, c).start()
+        keep_down(mirror, 2 * c)
 
     def down_far(c):
-        passing("down", far, c, partner).wait_recv()
-        share("down", far, g, c).start()
-
-    def down_partner(c, shared):
-        from_partner("down", c)
-        if shared:
-            share("down", pz, g, c).start()
+        keep_down(far, 2 * c)
+
+    def down_partner(c):
+        from_partner("down", 2 * c)
+        from_partner("down", 2 * c + 1)
 
     def first_ffn():
         for copy in local:
@@ -381,36 +432,41 @@
         from_mirror("gu", 7)
         from_partner("gu", 5)
         add_shard(1, z, True)
+        from_partner("gu", 6)
         settle("pool", mirror)
         spread_pool(mirror)
         from_far("pool", 0)
         from_far("gu", 0)
-        from_partner("gu", 6)
-        settle("gu", mirror, 0, 4)
+        settle("gate", mirror)
         add_shard(0, mirror)
+        from_partner("gu", 7)
+        pl.loop(0, 8)(lambda c: own_inward("down", c).start())
         from_far("gu", 1)
-        from_partner("gu", 7)
-        pl.loop(0, 4)(lambda c: own_inward("down", c).start())
-        settle("gu", mirror, 4, 8)
+        settle("up", mirror)
         add_shard(1, mirror)
-        pl.loop(2, 5)(lambda m: from_far("gu", m))
+        from_far("gu", 2)
         settle("pool", far)
         spread_pool(far)
+        from_far("gu", 3)
         settle("pool", pz)
         spread_pool(pz)
-        settle("gu", far, 0, 4)
+        from_far("gu", 4)
+        from_far("gu", 5)
+        settle("gate", far)
         add_shard(0, far)
-        from_far("gu", 5)
-        settle("gu", pz, 0, 4)
+        from_far("gu", 6)
+        settle("gate", pz)
         add_shard(0, pz)
-        pl.loop(6, 8)(lambda m: from_far("gu", m))
-        settle("gu", far, 4, 8)
-        add_shard(1, far)
+        from_far("gu", 7)
+        pl.loop(0, 4)(lambda c: own_partner("down", c).start())
         down_mirror(0)
         down_mirror(1)
-        settle("gu", pz, 4, 8)
+        settle("up", far)
+        add_shard(1, far)
+        settle("up", pz)
+        down_mirror(2)
+        down_partner(0)
         add_shard(1, pz)
-        down_mirror(2)
 
         @pl.loop(0, f_loc // tile)
         def _(i):
@@ -448,46 +504,49 @@
             res[0, mine, cols] = (tok_ref[mine, cols].astype(f32) + 0.5 * total).astype(jnp.bfloat16)
             final_copy(0, j, place, mine).start()
 
-        down_partner(0, False)
         down_mirror(3)
-        for j in range(n_blocks):
-            if j == 2:
-                down_partner(1, False)
-                down_far(0)
-                settle("down", mirror)
-            if j == 4:
-                down_partner(2, True)
-                down_far(1)
-                down_partner(3, True)
-                down_far(2)
-            if j == 5:
-                down_far(3)
-            if j == 6:
-                settle("down", pz)
-            if j == 7:
-                settle("down", far)
-            multiply(j)
-            if j >= 1:
-                add_pair(j - 1)
-            if j >= 3:
-                finish(j - 3)
-            if j == 5:
-                own_partner("down", 0).start()
-            if j == 7:
-                own_partner("down", 1).start()
-        add_pair(n_blocks - 1)
-        for j in range(n_blocks - 3, n_blocks):
-            finish(j)
-        own_partner("down", 2).start()
-        own_partner("down", 3).start()
-        pl.loop(0, 4)(lambda c: passing("down", mirror, c, partner).start())
-        pl.loop(0, 4)(lambda c: passing("down", far, c, partner).start())
-        for j in range(n_blocks):
-            final_copy(0, j, first_place(j, z), other).wait_recv()
+        down_partner(1)
+        multiply(0)
+        multiply(1)
+        add_pair(0)
+        down_far(0)
+        down_partner(2)
+        add_pair(1)
+        settle("down", mirror)
+        multiply(2)
+        multiply(3)
+        add_pair(2)
+        down_partner(3)
+        down_far(1)
+        multiply(4)
+        add_pair(3)
+        down_far(2)
+        add_pair(4)
+        finish(0)
+        finish(1)
+        down_far(3)
+        multiply(5)
+        finish(2)
+        add_pair(5)
+        finish(3)
+        pl.loop(4, 8)(lambda c: own_partner("down", c).start())
+        settle("down", pz)
+        multiply(6)
+        finish(4)
+        add_pair(6)
+        settle("down", far)
+        multiply(7)
+        finish(5)
+        add_pair(7)
+        finish(6)
+        finish(7)
+        pl.loop(0, 8)(lambda c: passing("down", mirror, c, partner).start())
+        pl.loop(0, 8)(lambda c: passing("down", far, c, partner).start())
+        final_all(0, other).wait_recv()
 
     def take(name, s, c):
-        passing(name, s, c, partner).wait_recv()
-        share(name, s, g, c).start()
+        arrival(name, s, c).wait_recv()
+        share(name, s, c).start()
 
     def collect():
         for copy in local:
@@ -501,20 +560,25 @@
 
         def hand_out(j):
             lend_copy(j, pz).wait_recv()
-            for off in range(1, n_tp):
-                lent_copy(j, off, t).start()
+            lent_copy(j, 1).start()
+            lent_copy(j, 0).start()
+
+        def hand_on(j):
+            lent_arrival(j).wait_recv()
+            lent_copy(j, 2).start()
 
         for j in range(n_blocks):
+            if j % 4 == 0:
+                pl.loop(j, j + 4)(lambda c: take("down", pz, c))
             hand_out(j)
-            if j == 2:
-                take("down", pz, 0)
-            if j == 4:
-                take("down", pz, 1)
-        for s in (pz, far, mirror):
-            settle("gu", s)
-        for j in range(n_blocks):
-            for off in range(1, n_tp):
-                lent_copy(j, off, lax.rem(t - off + n_tp, n_tp)).wait_recv()
+            if j >= 2:
+                hand_on(j - 2)
+        hand_on(n_blocks - 2)
+        hand_on(n_blocks - 1)
+        take("down", far, 0)
+        t_mate = t + 1 - 2 * core
+        lent_all(0, t_mate).wait_recv()
+        lent_all(2, lax.rem(t_mate + 2, n_tp)).wait_recv()
 
     pl.when(inner)(first_ffn)
     pl.when(outer)(collect)
@@ -522,10 +586,17 @@
     def when_outer(act):
         pl.when(outer)(act)
 
+    def take_down(s, low, high):
+        @pl.when(outer)
+        def _():
+            for c in range(low, high):
+                take("down", s, c)
+
+    take_down(far, 1, 2)
     norm_rows(res.at[0], gainm_ref)
+    take_down(far, 2, 3)
     for off in range(1, n_tp):
-        for s in range(n):
-            pool_copy(off, s, lax.rem(t - off + n_tp, n_tp)).wait_recv()
+        pool_all(off, lax.rem(t - off + n_tp, n_tp)).wait_recv()
     group_width = width // groups
     row_id = lax.broadcasted_iota(jnp.int32, (n_rows, n_rows), 0)
     col_id = lax.broadcasted_iota(jnp.int32, (n_rows, n_rows), 1)
@@ -542,10 +613,17 @@
         deviation = (mean - normed[own_seq, cols].astype(f32)).astype(jnp.bfloat16)
         mapped = jnp.dot(deviation, pool_full[k], preferred_element_type=f32) + bias_ref[pl.ds(k, 1), :]
         amix[:, cols] = (res[0, :, cols].astype(f32) + mapped * scale_ref[:, cols]).astype(jnp.bfloat16)
-        if k % 2 == 1:
-            when_outer(lambda: take("down", pz, 2 + k // 2))
+        if k == 1:
+            take_down(far, 3, 4)
 
     norm_rows(amix, gain2_ref)
+
+    @pl.when(outer)
+    def _():
+        for s in (pz, far, mirror):
+            settle("gate", s)
+            settle("up", s)
+        take("down", far, 4)
 
     @pl.loop(0, f_loc // tile)
     def _(i):
@@ -554,19 +632,19 @@
         up_proj = jnp.dot(normed[own_seq, :], gu_full[1, :, cols], preferred_element_type=f32)
         hidden[own_seq, cols] = activate(gate_proj, up_proj)
 
-        @pl.when(outer & (i < 4))
+        @pl.when(outer & (i % 2 == 0))
         def _():
-            take("down", far, i)
+            take("down", far, 5 + i // 2)
 
     def pair_copy(j):
-        return remote(part1.at[j, other, :], rbuf1.at[j], csend.at[1, j], crecv.at[1, j], mate)
+        return remote(part1.at[j, other, :], rbuf1.at[j], csend.at[1], crecv.at[1, j], mate)
 
     def x_copy(j):
-        return remote(xs1.at[j], xr1.at[j], xsend.at[1, j], xrecv.at[1, j], x_peer)
+        return remote(xs1.at[j], xr1.at[j], xsend.at[1], xrecv.at[1, j], x_peer)
 
     def out_copy(j):
         cols = columns(second_place(j))
-        return pltpu.make_async_copy(res.at[1, :, cols], out_ref.at[:, cols], osem.at[j])
+        return pltpu.make_async_copy(res.at[1, :, cols], out_ref.at[:, cols], osem.at[0])
 
     def multiply(j):
         s, half = second_place(j)
@@ -590,77 +668,100 @@
         final_copy(1, j, second_place(j), other).wait_recv()
         out_copy(j).start()
 
-    for j in range(n_blocks):
-        if j == 3:
-            when_outer(lambda: settle("down", pz))
-        if j == 5:
-            when_outer(lambda: settle("down", far))
-        if 3 <= j < 7:
-            when_outer(lambda: take("down", mirror, j - 3))
-        if j == 7:
-            when_outer(lambda: settle("down", mirror))
-        multiply(j)
-        if j >= 1:
-            add_pair(j - 1)
-        if j >= 3:
-            finish(j - 3)
-        if j >= 5:
-            emit(j - 5)
-    add_pair(n_blocks - 1)
-    for j in range(n_blocks - 3, n_blocks):
-        finish(j)
-    for j in range(n_blocks - 5, n_blocks):
-        emit(j)
-
-    @pl.loop(0, n)
-    def _(s):
+    def drain_early():
         for off in range(1, n_tp):
-            pool_copy(off, s, t).wait_send()
-
-    for name in ("pool", "gate", "up", "down"):
-        pl.loop(0, 1 if name == "pool" else 4)(lambda c: own_partner(name, c).wait_send())
+            pool_all(off, t).wait_send()
+        for name in kinds:
+            sent(name, z, g, zsend.at[z], partner).wait_send()
+
+        @pl.when(outer)
+        def _():
+            tok_copy.wait_send()
+            for name in kinds:
+                sent(name, z, 1 - g, ysend.at[z], partner).wait_send()
+                for s in (pz, far, mirror):
+                    if name != "down":
+                        sent(name, s, g, ysend.at[s], y_peer).wait_send()
+            sent("down", pz, g, ysend.at[pz], y_peer).wait_send()
+            for lane in range(3):
+                lent_all(lane, t).wait_send()
+
+        @pl.when(inner)
+        def _():
+            for off in range(1, n_tp):
+                guest_copy(off, t).wait_send()
+            for name in kinds:
+                sent(name, z, g, zleft, inward).wait_send()
+                sent(name, pz, g, zsend.at[pz], inward).wait_send()
+                for s in (mirror, far):
+                    sent(name, s, g, ysend.at[s], y_peer).wait_send()
+                    if name != "down":
+                        sent(name, s, g, zsend.at[s], partner).wait_send()
+            remote(rbuf0, rbuf0, csend.at[0], crecv.at[0, 0], mate).wait_send()
+            remote(xr0, xr0, xsend.at[0], xrecv.at[0, 0], x_peer).wait_send()
+            remote(xg0, xg0, gsend.at[0], grecv.at[0], x_peer).wait_send()
+            remote(lent, lent, asend.at[1], arecv.at[1], partner).wait_send()
+            final_all(0, mine).wait_send()
+
+    multiply(0)
+    take_down(mirror, 0, 1)
+    multiply(1)
+    add_pair(0)
+    multiply(2)
+    add_pair(1)
+    take_down(mirror, 1, 2)
+    when_outer(lambda: settle("down", pz))
+    multiply(3)
+    add_pair(2)
+    take_down(mirror, 2, 3)
+    multiply(4)
+    add_pair(3)
+    when_outer(lambda: settle("down", far))
+    multiply(5)
+    add_pair(4)
+    take_down(mirror, 3, 4)
+    finish(0)
+    take_down(mirror, 4, 5)
+    finish(1)
+    add_pair(5)
+    take_down(mirror, 5, 6)
+    drain_early()
+    finish(2)
+    emit(0)
+    take_down(mirror, 6, 7)
+    finish(3)
+    emit(1)
+    take_down(mirror, 7, 8)
+    multiply(6)
+    emit(2)
+    finish(4)
+    add_pair(6)
+    emit(3)
+    when_outer(lambda: settle("down", mirror))
+    multiply(7)
+    finish(5)
+    add_pair(7)
+    emit(4)
+    finish(6)
+    emit(5)
+    finish(7)
+    emit(6)
+    emit(7)
 
     @pl.when(outer)
     def _():
-        tok_copy.wait_send()
-        for name in ("pool", "gate", "up", "down"):
-            direct = {"pool": 1, "down": 2}.get(name, 4)
-            pl.loop(0, direct)(lambda c: own_direct(name, c).wait_send())
-        for s in (pz, far, mirror):
-            for name in ("pool", "gu", "down"):
-                each(name, lambda c: share(name, s, g, c).wait_send())
-        for j in range(n_blocks):
-            for off in range(1, n_tp):
-                lent_copy(j, off, t).wait_send()
+        for s in (far, mirror):
+            sent("down", s, g, ysend.at[s], y_peer).wait_send()
 
     @pl.when(inner)
     def _():
-        for off in range(1, n_tp):
-            guest_copy(off, t).wait_send()
-        for name in ("pool", "gate", "up", "down"):
-            pl.loop(0, 1 if name == "pool" else 4)(lambda c: own_inward(name, c).wait_send())
-        for name in ("pool", "gu", "down"):
-            each(name, lambda c: passing(name, pz, c, inward).wait_send())
-            for s in (mirror, far):
-
-                def sent(c):
-                    passing(name, s, c, partner).wait_send()
-                    share(name, s, g, c).wait_send()
-
-                each(name, sent)
-        pl.loop(2, 4)(lambda c: share("down", pz, g, c).wait_send())
-        for j in range(n_blocks):
-            pair_first(j).wait_send()
-            x_first(j).wait_send()
-            x_guest(j).wait_send()
-            lend_copy(j, z).wait_send()
-            final_copy(0, j, first_place(j, z), mine).wait_send()
-
-    for j in range(n_blocks):
-        pair_copy(j).wait_send()
-        x_copy(j).wait_send()
-        final_copy(1, j, second_place(j), mine).wait_send()
-        out_copy(j).wait()
+        for s in (mirror, far):
+            sent("down", s, g, zsend.at[s], partner).wait_send()
+
+    remote(xr1, xr1, csend.at[1], crecv.at[1, 0], mate).wait_send()
+    remote(xr1, xr1, xsend.at[1], xrecv.at[1, 0], x_peer).wait_send()
+    final_all(1, mine).wait_send()
+    pltpu.make_async_copy(res.at[1], out_ref, osem.at[0]).wait()
 
 
 def fused_shards(
@@ -699,11 +800,11 @@
             vmem((blocks, half, block), bf16),
             vmem((blocks, half, block), bf16),
             vmem((blocks, half, block), bf16),
-            dma((n, 13)), dma((13,)), dma((n, 13)), dma((n, 13)), dma((n, 13)),
-            dma((n_tp - 1, n)), dma((n_tp - 1, n)), dma((5,)),
-            dma((1 + blocks,)), dma((1 + blocks,)), dma((n_tp - 1, 1 + blocks)), dma((n_tp - 1, 1 + blocks)),
-            dma((2, blocks)), dma((2, blocks)), dma((2, blocks)), dma((2, blocks)), dma((blocks,)), dma((blocks,)),
-            dma((2, blocks)), dma((2, blocks)), dma((blocks,)),
+            dma((n, 3)), dma((3,)), dma((n - 1, 17)), dma((n, 3)), dma((n - 1, 4)),
+            dma((n_tp - 1,)), dma((n_tp - 1,)), dma((5,)),
+            dma((2,)), dma((1 + blocks,)), dma((6,)), dma((5 + blocks,)),
+            dma((2,)), dma((2, blocks)), dma((2,)), dma((2, blocks)), dma((1,)), dma((blocks,)),
+            dma((2,)), dma((1 + blocks,)), dma((1,)),
         ],
         compiler_params=pltpu.CompilerParams(
             collective_id=0, has_side_effects=True, vmem_limit_bytes=60 * 1024 * 1024
@@ -719,7 +820,7 @@
     d_loc, f_loc = args[1].shape
     pool_rows, _, pool_cols = args[4].shape
     fits = n_grp == 2 and n_tp == 4 and n == 4 and n_rows % 64 == 0
-    fits = fits and d_loc % 512 == 0 and f_loc % 256 == 0 and pool_rows % 32 == 0 and pool_cols % 128 == 0
+    fits = fits and d_loc % 512 == 0 and f_loc % 1280 == 0 and pool_rows % 32 == 0 and pool_cols % 128 == 0
     return fused_shards(n, n_tp, *args) if fits else shards(*args)
 
 

time: 186 us -> 166 us (0.89)
  Pallas kernels: 181 us -> 162 us
    pallas_call x1, Pallas kernels: 181 us -> 162 us  [fused_shards(): pl.pallas_call(functools.partial(fused_kernel, (n, n_tp)), out_shape=jax....]
where the time goes in v2:
time: 166 us
  Pallas kernels  162 us (98%)
  local copies, waits for them, and re-layouts  4.3 us (3%)
    pallas_call x1, Pallas kernels, fused_shards(): pl.pallas_call(functools.partial(fused_kernel, (n, n_tp)), out_shape=jax....  162 us
    unnamed x2, local copies, waits for them, and re-layouts  4.3 us

profile of v2, /device:TPU:0, one launch (start us, length us, event | category | flops | bytes accessed | tf_op | source)
XLA Modules:
  0.0 166.2 jit_solution(5497212179940978011)
XLA Ops:
  0.0 1.6 copy.13
  1.6 161.9 %shard_map.100 = bf16[384,2048]{1,0:T(8,128)(2,1)} custom-call(bf16[384,2048]{1,0:T(8,128)(2,1)} %tok_ref.1, bf16[512,1280]{1,0:T(8,128)(2,1)} %gate_ref.1, bf16[512,1280]{1,0:T(8,128)(2,1)} %up_ref.1, bf16[1280,512]{1,0:T(8,128)(2,1)} %down_ref.1, bf16[4,128,128]{2,1,0:T(8,128)(2,1)} %bitcast.7, f32[4,512]{1,0:T(4,128)} %bias_ref.1, f32[1,2048]{1,0:T(1,128)} %bitcast.8, ...), custom_call_target="tpu_custom_call" | custom-call | tf_op jit(solution)/shard_map/pallas_call | solution.py:778
  163.5 2.7 %copy.15 = bf16[384,2048]{1,0:T(8,128)(2,1)} copy(bf16[384,2048]{1,0:T(8,128)(2,1)} %shard_map.100) | data formatting | bytes 3145728

commit v3 on v2

--- a/solution.py
+++ b/solution.py
@@ -96,10 +96,10 @@
 
 
 def fused_kernel(
-    sizes, tok_ref, gate_ref, up_ref, down_ref, pool_ref, bias_ref, scale_ref, gain1_ref, gainm_ref, gain2_ref,
+    sizes, tok_hbm, gate_ref, up_ref, down_ref, pool_hbm, bias_hbm, scale_hbm, gain1_hbm, gainm_hbm, gain2_hbm,
     out_ref,
     gu_full, down_full, pool_full, acc, normed, hidden, amix, res, guest, part0, rbuf0, xs0, xr0, xg0, lent,
-    part1, rbuf1, xs1, xr1,
+    part1, rbuf1, xs1, xr1, tok_ref, pool_ref, bias_ref, scale_ref, gain1_ref, gainm_ref, gain2_ref,
     zsend, zleft, zrecv, ysend, yrecv, tsend, trecv, lsem, asend, arecv, qsend, qrecv,
     csend, crecv, xsend, xrecv, gsend, grecv, fsend, frecv, osem,
 ):
@@ -113,12 +113,13 @@
     mirror, far = n - 1 - z, n - 1 - pz
     y_peer, partner, inward = {"grp": 1 - g}, {"fs": pz}, {"fs": mirror}
     mate, x_peer = {"tp": t + 1 - 2 * core}, {"tp": lax.rem(t + 2, n_tp)}
-    n_rows, width = tok_ref.shape
+    n_rows, width = tok_hbm.shape
     d_loc, f_loc = gate_ref.shape
-    groups, pool_rows, pool_cols = pool_ref.shape
+    pool_rows, groups, pool_cols = pool_hbm.shape
     half_rows = n_rows // 2
     quarter = n_rows // n_tp
     block_cols = d_loc // 2
+    sub_cols = block_cols // 2
     n_blocks = 2 * n
     f32 = jnp.float32
 
@@ -161,12 +162,13 @@
         return lax.rem(s - at + n, n) - 1
 
     def bulk(name, c):
-        return 0 if name == "pool" else 3 if name == "down" else 1 + c // 4
+        return 0 if name == "pool" else (3 if name == "down" else 1) + c // 4
 
     def region(name, s, half, c):
         if name == "down":
-            size = f_loc // 8
-            return down_full.at[s, half, pl.ds(pl.multiple_of(c * size, 16), size), :]
+            size = f_loc // 4
+            rows = pl.ds(pl.multiple_of(lax.rem(c, 4) * size, 16), size)
+            return down_full.at[s, half, rows, pl.ds(pl.multiple_of(c // 4 * sub_cols, 128), sub_cols)]
         if name == "pool":
             size = pool_rows // 2
             rows = pl.ds(pl.multiple_of(s * pool_rows + half * size, 16), size)
@@ -185,12 +187,11 @@
 
     def source(name, half, c):
         if name == "down":
-            size = f_loc // 8
-            cols = pl.ds(pl.multiple_of(half * block_cols, 128), block_cols)
-            return down_ref.at[pl.ds(pl.multiple_of(c * size, 16), size), cols]
+            size = f_loc // 4
+            cols = pl.ds(pl.multiple_of(half * block_cols + c // 4 * sub_cols, 128), sub_cols)
+            return down_ref.at[pl.ds(pl.multiple_of(lax.rem(c, 4) * size, 16), size), cols]
         if name == "pool":
-            size = pool_rows // 2
-            return pool_ref.at[:, pl.ds(pl.multiple_of(half * size, 16), size), :]
+            return region(name, z, half, c)
         size = d_loc // 8
         rows = pl.ds(pl.multiple_of(half * (d_loc // 2) + c * size, 16), size)
         return {"gate": gate_ref, "up": up_ref}[name].at[rows, :]
@@ -224,9 +225,17 @@
         return remote(there, there, ysend.at[s, kind[name]], yrecv.at[slot(s, z), bulk(name, c)], y_peer)
 
     def settle(name, s):
+        if name == "down":
+            settle_down(s, 0)
+            settle_down(s, 1)
+            return
         there = whole(name, s, 1 - g)
-        where = {"pool": 0, "gate": 1, "up": 2, "down": 3}[name]
+        where = {"pool": 0, "gate": 1, "up": 2}[name]
         remote(there, there, ysend.at[s, 0], yrecv.at[slot(s, z), where], y_peer).wait_recv()
+
+    def settle_down(s, part):
+        there = down_full.at[s, 1 - g, :, pl.ds(part * sub_cols, sub_cols)]
+        remote(there, there, ysend.at[s, 0], yrecv.at[slot(s, z), 3 + part], y_peer).wait_recv()
 
     def sent(name, s, half, sems, dev):
         there = whole(name, s, half)
@@ -244,39 +253,57 @@
             pl.loop(0, own_counts[name])(lambda c: make(name, c).start())
 
     tok_copy = remote(
-        tok_ref.at[quarter_rows(t), :], guest.at[quarter_rows(t), :], asend.at[0], arecv.at[0], partner
+        tok_hbm.at[quarter_rows(t), :], guest.at[quarter_rows(t), :], asend.at[0], arecv.at[0], partner
     )
+
+    own_rows = pl.ds(pl.multiple_of(z * d_loc, 128), d_loc)
+    pool_in = pltpu.make_async_copy(pool_hbm, pool_ref, lsem.at[0])
+    local = [
+        pltpu.make_async_copy(tok_hbm, tok_ref, lsem.at[1]),
+        pltpu.make_async_copy(gate_ref, gu_full.at[0, own_rows, :], lsem.at[2]),
+        pltpu.make_async_copy(up_ref, gu_full.at[1, own_rows, :], lsem.at[3]),
+        pltpu.make_async_copy(down_ref.at[:, pl.ds(0, block_cols)], down_full.at[z, 0], lsem.at[4]),
+        pltpu.make_async_copy(down_ref.at[:, pl.ds(block_cols, block_cols)], down_full.at[z, 1], lsem.at[5]),
+        pltpu.make_async_copy(bias_hbm, bias_ref, lsem.at[6]),
+        pltpu.make_async_copy(scale_hbm, scale_ref, lsem.at[7]),
+        pltpu.make_async_copy(gain1_hbm, gain1_ref, lsem.at[8]),
+        pltpu.make_async_copy(gainm_hbm, gainm_ref, lsem.at[9]),
+        pltpu.make_async_copy(gain2_hbm, gain2_ref, lsem.at[10]),
+    ]
+    pool_in.start()
 
     @pl.when(outer)
     def _():
         tok_copy.start()
-        start_each(("pool", "gate", "up"), own_partner)
-        start_each(("pool", "gate", "up"), own_direct)
-        start_each(("down",), own_partner)
-        start_each(("down",), own_direct)
+        start_each(("gate", "up"), own_partner)
 
     @pl.when(inner)
     def _():
-        for name in ("pool", "gate", "up"):
-
-            @pl.loop(0, own_counts[name])
+        for name in ("gate", "up"):
+
+            @pl.loop(0, 4)
             def _(c):
                 own_inward(name, c).start()
                 own_partner(name, c).start()
 
-    own_rows = pl.ds(pl.multiple_of(z * d_loc, 128), d_loc)
-    own_pool = pool_full.at[
-        :, pl.ds(pl.multiple_of(z * pool_rows, 16), pool_rows), pl.ds(pl.multiple_of(t * pool_cols, 128), pool_cols)
-    ]
-    local = [
-        pltpu.make_async_copy(pool_ref, own_pool, lsem.at[0]),
-        pltpu.make_async_copy(gate_ref, gu_full.at[0, own_rows, :], lsem.at[1]),
-        pltpu.make_async_copy(up_ref, gu_full.at[1, own_rows, :], lsem.at[2]),
-        pltpu.make_async_copy(down_ref.at[:, pl.ds(0, block_cols)], down_full.at[z, 0], lsem.at[3]),
-        pltpu.make_async_copy(down_ref.at[:, pl.ds(block_cols, block_cols)], down_full.at[z, 1], lsem.at[4]),
-    ]
     for copy in local:
         copy.start()
+    pool_in.wait()
+    for k in range(groups):
+        pool_full[
+            k, pl.ds(pl.multiple_of(z * pool_rows, 16), pool_rows), pl.ds(pl.multiple_of(t * pool_cols, 128), pool_cols)
+        ] = pool_ref[:, k, :]
+    own_partner("pool", 0).start()
+
+    @pl.when(outer)
+    def _():
+        start_each(("gate", "up", "pool"), own_direct)
+        start_each(("down",), own_partner)
+        start_each(("down",), own_direct)
+
+    @pl.when(inner)
+    def _():
+        own_inward("pool", 0).start()
 
     def norm_rows(src, gain, base=0):
         @pl.loop(0, n_rows // 32)
@@ -335,7 +362,7 @@
 
     def final_copy(phase, j, place, rows):
         there = res.at[phase, rows, columns(place)]
-        return remote(there, there, fsend.at[phase], frecv.at[phase * (1 + j)], mate)
+        return remote(there, there, fsend.at[phase], frecv.at[0], mate)
 
     def final_all(phase, rows):
         there = res.at[phase, rows, :]
@@ -413,10 +440,8 @@
         tok_copy.wait_recv()
         for off in range(1, n_tp):
             guest_copy(off, t).start()
-        from_mirror("pool", 0)
         from_mirror("gu", 0)
         from_mirror("gu", 1)
-        from_partner("pool", 0)
 
         @pl.loop(0, 4)
         def _(m):
@@ -432,24 +457,21 @@
         from_mirror("gu", 7)
         from_partner("gu", 5)
         add_shard(1, z, True)
+        from_mirror("pool", 0)
         from_partner("gu", 6)
-        settle("pool", mirror)
-        spread_pool(mirror)
-        from_far("pool", 0)
         from_far("gu", 0)
         settle("gate", mirror)
         add_shard(0, mirror)
         from_partner("gu", 7)
+        from_partner("pool", 0)
         pl.loop(0, 8)(lambda c: own_inward("down", c).start())
         from_far("gu", 1)
         settle("up", mirror)
         add_shard(1, mirror)
         from_far("gu", 2)
-        settle("pool", far)
-        spread_pool(far)
+        settle("pool", mirror)
+        spread_pool(mirror)
         from_far("gu", 3)
-        settle("pool", pz)
-        spread_pool(pz)
         from_far("gu", 4)
         from_far("gu", 5)
         settle("gate", far)
@@ -458,9 +480,12 @@
         settle("gate", pz)
         add_shard(0, pz)
         from_far("gu", 7)
+        from_far("pool", 0)
         pl.loop(0, 4)(lambda c: own_partner("down", c).start())
         down_mirror(0)
         down_mirror(1)
+        settle("pool", far)
+        spread_pool(far)
         settle("up", far)
         add_shard(1, far)
         settle("up", pz)
@@ -492,17 +517,24 @@
             x_guest(j).start()
             x_first(j).start()
 
-        def finish(j):
+        def lend(j):
+            x_guest(j).wait_recv()
+            total = xs0[j, 1, kept, :].astype(f32) + xg0[j].astype(f32)
+            cols = columns(first_place(j, z))
+            lent[j] = (guest[quarter_rows(t), cols].astype(f32) + 0.5 * total).astype(jnp.bfloat16)
+            lend_copy(j, z).start()
+
+        def keep(j):
+            x_first(j).wait_recv()
             place = first_place(j, z)
             cols = columns(place)
-            x_guest(j).wait_recv()
-            total = xs0[j, 1, kept, :].astype(f32) + xg0[j].astype(f32)
-            lent[j] = (guest[quarter_rows(t), cols].astype(f32) + 0.5 * total).astype(jnp.bfloat16)
-            lend_copy(j, z).start()
-            x_first(j).wait_recv()
             total = xs0[j, 0].astype(f32) + xr0[j].astype(f32)
             res[0, mine, cols] = (tok_ref[mine, cols].astype(f32) + 0.5 * total).astype(jnp.bfloat16)
             final_copy(0, j, place, mine).start()
+
+        def finish(j):
+            lend(j)
+            keep(j)
 
         down_mirror(3)
         down_partner(1)
@@ -529,19 +561,25 @@
         finish(2)
         add_pair(5)
         finish(3)
-        pl.loop(4, 8)(lambda c: own_partner("down", c).start())
         settle("down", pz)
         multiply(6)
         finish(4)
+        pl.loop(4, 6)(lambda c: own_partner("down", c).start())
         add_pair(6)
         settle("down", far)
         multiply(7)
-        finish(5)
+        lend(5)
         add_pair(7)
-        finish(6)
-        finish(7)
+        settle("pool", pz)
+        spread_pool(pz)
+        keep(5)
+        lend(6)
+        lend(7)
+        pl.loop(6, 8)(lambda c: own_partner("down", c).start())
         pl.loop(0, 8)(lambda c: passing("down", mirror, c, partner).start())
         pl.loop(0, 8)(lambda c: passing("down", far, c, partner).start())
+        keep(6)
+        keep(7)
         final_all(0, other).wait_recv()
 
     def take(name, s, c):
@@ -552,11 +590,13 @@
         for copy in local:
             copy.wait()
         spread_pool(z)
-        for s in (pz, far, mirror):
+        shards_in = (pz, far, mirror)
+        for i, s in enumerate(shards_in):
+            pl.loop(0, 8)(lambda m: take("gu", s, m))
             take("pool", s, 0)
-            pl.loop(0, 8)(lambda m: take("gu", s, m))
-            settle("pool", s)
-            spread_pool(s)
+            if i > 0:
+                settle("pool", shards_in[i - 1])
+                spread_pool(shards_in[i - 1])
 
         def hand_out(j):
             lend_copy(j, pz).wait_recv()
@@ -567,15 +607,24 @@
             lent_arrival(j).wait_recv()
             lent_copy(j, 2).start()
 
-        for j in range(n_blocks):
-            if j % 4 == 0:
-                pl.loop(j, j + 4)(lambda c: take("down", pz, c))
+        pl.loop(0, 3)(lambda c: take("down", pz, c))
+        settle("pool", mirror)
+        spread_pool(mirror)
+        take("down", pz, 3)
+        for j in range(5):
             hand_out(j)
-            if j >= 2:
-                hand_on(j - 2)
-        hand_on(n_blocks - 2)
-        hand_on(n_blocks - 1)
-        take("down", far, 0)
+        pl.loop(4, 6)(lambda c: take("down", pz, c))
+        for j in range(4):
+            hand_on(j)
+        hand_out(5)
+        hand_on(4)
+        hand_out(6)
+        hand_out(7)
+        hand_on(5)
+        hand_on(6)
+        take("down", pz, 6)
+        hand_on(7)
+        take("down", pz, 7)
         t_mate = t + 1 - 2 * core
         lent_all(0, t_mate).wait_recv()
         lent_all(2, lax.rem(t_mate + 2, n_tp)).wait_recv()
@@ -592,9 +641,8 @@
             for c in range(low, high):
                 take("down", s, c)
 
-    take_down(far, 1, 2)
     norm_rows(res.at[0], gainm_ref)
-    take_down(far, 2, 3)
+    take_down(far, 0, 1)
     for off in range(1, n_tp):
         pool_all(off, lax.rem(t - off + n_tp, n_tp)).wait_recv()
     group_width = width // groups
@@ -613,8 +661,8 @@
         deviation = (mean - normed[own_seq, cols].astype(f32)).astype(jnp.bfloat16)
         mapped = jnp.dot(deviation, pool_full[k], preferred_element_type=f32) + bias_ref[pl.ds(k, 1), :]
         amix[:, cols] = (res[0, :, cols].astype(f32) + mapped * scale_ref[:, cols]).astype(jnp.bfloat16)
-        if k == 1:
-            take_down(far, 3, 4)
+        if k % 2 == 1:
+            take_down(far, 1 + k // 2, 2 + k // 2)
 
     norm_rows(amix, gain2_ref)
 
@@ -623,7 +671,7 @@
         for s in (pz, far, mirror):
             settle("gate", s)
             settle("up", s)
-        take("down", far, 4)
+        take("down", far, 3)
 
     @pl.loop(0, f_loc // tile)
     def _(i):
@@ -632,41 +680,52 @@
         up_proj = jnp.dot(normed[own_seq, :], gu_full[1, :, cols], preferred_element_type=f32)
         hidden[own_seq, cols] = activate(gate_proj, up_proj)
 
-        @pl.when(outer & (i % 2 == 0))
+        @pl.when(outer & (i % 2 == 1))
         def _():
-            take("down", far, 5 + i // 2)
-
-    def pair_copy(j):
-        return remote(part1.at[j, other, :], rbuf1.at[j], csend.at[1], crecv.at[1, j], mate)
-
-    def x_copy(j):
-        return remote(xs1.at[j], xr1.at[j], xsend.at[1], xrecv.at[1, j], x_peer)
-
-    def out_copy(j):
-        cols = columns(second_place(j))
-        return pltpu.make_async_copy(res.at[1, :, cols], out_ref.at[:, cols], osem.at[0])
-
-    def multiply(j):
-        s, half = second_place(j)
-        part1[j] = jnp.dot(hidden[own_seq, :], down_full[s, half], preferred_element_type=f32).astype(jnp.bfloat16)
-        pair_copy(j).start()
-
-    def add_pair(j):
-        pair_copy(j).wait_recv()
-        xs1[j] = (part1[j, mine, :].astype(f32) + rbuf1[j].astype(f32)).astype(jnp.bfloat16)
-        x_copy(j).start()
-
-    def finish(j):
-        x_copy(j).wait_recv()
-        place = second_place(j)
-        cols = columns(place)
-        total = xs1[j].astype(f32) + xr1[j].astype(f32)
+            take("down", far, 4 + i // 2)
+
+    def spot(b):
+        place, wide = second_place(min(b, n_blocks - 1)), b < n_blocks - 1
+        off = 0 if wide else (b - n_blocks + 1) * sub_cols
+        size = block_cols if wide else sub_cols
+        cols = pl.ds(pl.multiple_of(place[0] * d_loc + place[1] * block_cols + off, 128), size)
+        return min(b, n_blocks - 1), place, cols, pl.ds(off, size)
+
+    def pair_copy(b):
+        j, _, _, lanes = spot(b)
+        return remote(part1.at[j, other, lanes], rbuf1.at[j, :, lanes], csend.at[1], crecv.at[1, b], mate)
+
+    def x_copy(b):
+        j, _, _, lanes = spot(b)
+        return remote(xs1.at[j, :, lanes], xr1.at[j, :, lanes], xsend.at[1], xrecv.at[1, b], x_peer)
+
+    def last_copy(b, rows):
+        there = res.at[1, rows, spot(b)[2]]
+        return remote(there, there, fsend.at[1], frecv.at[1 + b], mate)
+
+    def multiply(b):
+        j, (s, half), _, lanes = spot(b)
+        product = jnp.dot(hidden[own_seq, :], down_full[s, half, :, lanes], preferred_element_type=f32)
+        part1[j, :, lanes] = product.astype(jnp.bfloat16)
+        pair_copy(b).start()
+
+    def add_pair(b):
+        j, _, _, lanes = spot(b)
+        pair_copy(b).wait_recv()
+        xs1[j, :, lanes] = (part1[j, mine, lanes].astype(f32) + rbuf1[j, :, lanes].astype(f32)).astype(jnp.bfloat16)
+        x_copy(b).start()
+
+    def finish(b):
+        j, _, cols, lanes = spot(b)
+        x_copy(b).wait_recv()
+        total = xs1[j, :, lanes].astype(f32) + xr1[j, :, lanes].astype(f32)
         res[1, mine, cols] = (amix[mine, cols].astype(f32) + 0.5 * total).astype(jnp.bfloat16)
-        final_copy(1, j, place, mine).start()
-
-    def emit(j):
-        final_copy(1, j, second_place(j), other).wait_recv()
-        out_copy(j).start()
+        last_copy(b, mine).start()
+
+    def emit(b):
+        cols = spot(b)[2]
+        last_copy(b, other).wait_recv()
+        pltpu.make_async_copy(res.at[1, :, cols], out_ref.at[:, cols], osem.at[0]).start()
 
     def drain_early():
         for off in range(1, n_tp):
@@ -704,49 +763,55 @@
             final_all(0, mine).wait_send()
 
     multiply(0)
-    take_down(mirror, 0, 1)
+    take_down(far, 6, 7)
     multiply(1)
     add_pair(0)
     multiply(2)
     add_pair(1)
-    take_down(mirror, 1, 2)
+    take_down(far, 7, 8)
     when_outer(lambda: settle("down", pz))
     multiply(3)
     add_pair(2)
-    take_down(mirror, 2, 3)
     multiply(4)
     add_pair(3)
+    take_down(mirror, 0, 1)
+    add_pair(4)
+    take_down(mirror, 1, 3)
     when_outer(lambda: settle("down", far))
     multiply(5)
-    add_pair(4)
     take_down(mirror, 3, 4)
+    add_pair(5)
     finish(0)
     take_down(mirror, 4, 5)
+    drain_early()
     finish(1)
-    add_pair(5)
+    emit(0)
     take_down(mirror, 5, 6)
-    drain_early()
     finish(2)
-    emit(0)
+    emit(1)
     take_down(mirror, 6, 7)
     finish(3)
-    emit(1)
+    emit(2)
     take_down(mirror, 7, 8)
     multiply(6)
-    emit(2)
+    emit(3)
+    add_pair(6)
     finish(4)
-    add_pair(6)
-    emit(3)
-    when_outer(lambda: settle("down", mirror))
+    when_outer(lambda: settle_down(mirror, 0))
     multiply(7)
     finish(5)
     add_pair(7)
     emit(4)
+    when_outer(lambda: settle_down(mirror, 1))
+    multiply(8)
     finish(6)
+    add_pair(8)
     emit(5)
     finish(7)
     emit(6)
+    finish(8)
     emit(7)
+    emit(8)
 
     @pl.when(outer)
     def _():
@@ -770,20 +835,19 @@
 ):
     n_rows, width = tokens.shape
     d_loc, f_loc = gate_weight.shape
-    groups = pool_weight.shape[1]
-    pool = jnp.swapaxes(pool_weight, 0, 1)
+    pool_rows, groups, pool_cols = pool_weight.shape
     bf16, dma, vmem = jnp.bfloat16, pltpu.SemaphoreType.DMA, pltpu.VMEM
-    in_vmem, anywhere = pl.BlockSpec(memory_space=pltpu.VMEM), pl.BlockSpec(memory_space=pl.ANY)
+    anywhere = pl.BlockSpec(memory_space=pl.ANY)
     half, quarter, block, blocks = n_rows // 2, n_rows // n_tp, d_loc // 2, 2 * n
     return pl.pallas_call(
         functools.partial(fused_kernel, (n, n_tp)),
         out_shape=jax.ShapeDtypeStruct((n_rows, width), bf16),
-        in_specs=[in_vmem] + [anywhere] * 4 + [in_vmem] * 5,
+        in_specs=[anywhere] * 10,
         out_specs=anywhere,
         scratch_shapes=[
             vmem((2, n * d_loc, f_loc), bf16),
             vmem((n, 2, f_loc, block), bf16),
-            vmem((groups, n * pool.shape[1], n_tp * pool.shape[2]), bf16),
+            vmem((groups, n * pool_rows, n_tp * pool_cols), bf16),
             vmem((2, 2 * n_rows, f_loc), jnp.float32),
             vmem((2 * n_rows, width), bf16),
             vmem((2 * n_rows, f_loc), bf16),
@@ -800,17 +864,24 @@
             vmem((blocks, half, block), bf16),
             vmem((blocks, half, block), bf16),
             vmem((blocks, half, block), bf16),
-            dma((n, 3)), dma((3,)), dma((n - 1, 17)), dma((n, 3)), dma((n - 1, 4)),
-            dma((n_tp - 1,)), dma((n_tp - 1,)), dma((5,)),
+            vmem((n_rows, width), bf16),
+            vmem((pool_rows, groups, pool_cols), bf16),
+            vmem(pool_bias.shape, jnp.float32),
+            vmem((1, width), jnp.float32),
+            vmem((1, width), jnp.float32),
+            vmem((1, width), jnp.float32),
+            vmem((1, width), jnp.float32),
+            dma((n, 3)), dma((3,)), dma((n - 1, 17)), dma((n, 3)), dma((n - 1, 5)),
+            dma((n_tp - 1,)), dma((n_tp - 1,)), dma((11,)),
             dma((2,)), dma((1 + blocks,)), dma((6,)), dma((5 + blocks,)),
-            dma((2,)), dma((2, blocks)), dma((2,)), dma((2, blocks)), dma((1,)), dma((blocks,)),
-            dma((2,)), dma((1 + blocks,)), dma((1,)),
+            dma((2,)), dma((2, blocks + 1)), dma((2,)), dma((2, blocks + 1)), dma((1,)), dma((blocks,)),
+            dma((2,)), dma((2 + blocks,)), dma((1,)),
         ],
         compiler_params=pltpu.CompilerParams(
             collective_id=0, has_side_effects=True, vmem_limit_bytes=60 * 1024 * 1024
         ),
     )(
-        tokens, gate_weight, up_weight, down_weight, pool, pool_bias, pool_scale.reshape(1, width),
+        tokens, gate_weight, up_weight, down_weight, pool_weight, pool_bias, pool_scale.reshape(1, width),
         gain_first.reshape(1, width), gain_mix.reshape(1, width), gain_second.reshape(1, width),
     )
 

time: 166 us -> 161 us (0.970)
  Pallas kernels: 162 us -> 158 us
    pallas_call x1, Pallas kernels: 162 us -> 158 us  [fused_shards(): pl.pallas_call(functools.partial(fused_kernel, (n, n_tp)), out_shape=jax....]
    unnamed x2 -> x1, local copies, waits for them, and re-layouts: 4.3 us -> 2.73 us
where the time goes in v3:
time: 161 us
  Pallas kernels  158 us (98%)
  local copies, waits for them, and re-layouts  2.73 us (2%)
    pallas_call x1, Pallas kernels, fused_shards(): pl.pallas_call(functools.partial(fused_kernel, (n, n_tp)), out_shape=jax....  158 us

profile of v3, /device:TPU:0, one launch (start us, length us, event | category | flops | bytes accessed | tf_op | source)
XLA Modules:
  0.0 160.9 jit_solution(10579441588431090027)
XLA Ops:
  0.0 158.2 %shard_map.100 = bf16[384,2048]{1,0:T(8,128)(2,1)} custom-call(bf16[384,2048]{1,0:T(8,128)(2,1)} %tok_hbm.1, bf16[512,1280]{1,0:T(8,128)(2,1)} %gate_ref.1, bf16[512,1280]{1,0:T(8,128)(2,1)} %up_ref.1, bf16[1280,512]{1,0:T(8,128)(2,1)} %down_ref.1, bf16[128,4,128]{2,1,0:T(4,128)(2,1)} %pool_hbm.1, f32[4,512]{1,0:T(4,128)} %bias_hbm.1, f32[1,2048]{1,0:T(1,128)} %bitcast.4, ...), custom_call_target="tpu_custom_call" | custom-call | tf_op jit(solution)/shard_map/pallas_call | solution.py:842
  158.2 2.7 %copy.12 = bf16[384,2048]{1,0:T(8,128)(2,1)} copy(bf16[384,2048]{1,0:T(8,128)(2,1)} %shard_map.100) | data formatting | bytes 3145728

commit v4 on v3

--- a/solution.py
+++ b/solution.py
@@ -222,7 +222,17 @@
 
     def share(name, s, c):
         there = region(name, s, g, c)
-        return remote(there, there, ysend.at[s, kind[name]], yrecv.at[slot(s, z), bulk(name, c)], y_peer)
+        where = kind[name] + (c // 4 if name == "down" else 0)
+        return remote(there, there, ysend.at[s, where], yrecv.at[slot(s, z), bulk(name, c)], y_peer)
+
+    def shared(name, s, rows=None):
+        if name != "down":
+            sent(name, s, g, ysend.at[s], y_peer).wait_send()
+            return
+        for part in range(2):
+            size = f_loc if part == 0 or rows is None else rows
+            there = down_full.at[s, g, pl.ds(0, size), pl.ds(part * sub_cols, sub_cols)]
+            remote(there, there, ysend.at[s, 2 + part], yrecv.at[0, 0], y_peer).wait_send()
 
     def settle(name, s):
         if name == "down":
@@ -233,13 +243,17 @@
         where = {"pool": 0, "gate": 1, "up": 2}[name]
         remote(there, there, ysend.at[s, 0], yrecv.at[slot(s, z), where], y_peer).wait_recv()
 
-    def settle_down(s, part):
-        there = down_full.at[s, 1 - g, :, pl.ds(part * sub_cols, sub_cols)]
+    def settle_down(s, part, rows=None):
+        there = down_full.at[s, 1 - g, pl.ds(0, rows or f_loc), pl.ds(part * sub_cols, sub_cols)]
         remote(there, there, ysend.at[s, 0], yrecv.at[slot(s, z), 3 + part], y_peer).wait_recv()
 
     def sent(name, s, half, sems, dev):
         there = whole(name, s, half)
         return remote(there, there, sems.at[kind[name]], yrecv.at[0, 0], dev)
+
+    def extra_copy(s, at, dev):
+        there = region("down", s, 1 - g, 7)
+        return remote(there, there, zsend.at[s, 3], yrecv.at[slot(s, at), 5], dev)
 
     kinds = ("pool", "gu", "down")
 
@@ -578,6 +592,7 @@
         pl.loop(6, 8)(lambda c: own_partner("down", c).start())
         pl.loop(0, 8)(lambda c: passing("down", mirror, c, partner).start())
         pl.loop(0, 8)(lambda c: passing("down", far, c, partner).start())
+        extra_copy(far, pz, partner).start()
         keep(6)
         keep(7)
         final_all(0, other).wait_recv()
@@ -685,11 +700,12 @@
             take("down", far, 4 + i // 2)
 
     def spot(b):
-        place, wide = second_place(min(b, n_blocks - 1)), b < n_blocks - 1
-        off = 0 if wide else (b - n_blocks + 1) * sub_cols
-        size = block_cols if wide else sub_cols
+        wide = b < n_blocks - 2
+        j = b if wide else n_blocks - 2 + b % 2
+        place = second_place(j)
+        off, size = (0, block_cols) if wide else ((b - n_blocks + 2) // 2 * sub_cols, sub_cols)
         cols = pl.ds(pl.multiple_of(place[0] * d_loc + place[1] * block_cols + off, 128), size)
-        return min(b, n_blocks - 1), place, cols, pl.ds(off, size)
+        return j, place, cols, pl.ds(off, size)
 
     def pair_copy(b):
         j, _, _, lanes = spot(b)
@@ -707,6 +723,19 @@
         j, (s, half), _, lanes = spot(b)
         product = jnp.dot(hidden[own_seq, :], down_full[s, half, :, lanes], preferred_element_type=f32)
         part1[j, :, lanes] = product.astype(jnp.bfloat16)
+        pair_copy(b).start()
+
+    early_rows = f_loc // 4 * 3 // 128 * 128
+
+    def multiply_last(b):
+        j, (s, half), _, lanes = spot(b)
+        early, late = pl.ds(0, early_rows), pl.ds(early_rows, f_loc - early_rows)
+        when_outer(lambda: settle_down(mirror, 1, f_loc // 4 * 3))
+        held = acc.at[0, own_seq, pl.ds(0, sub_cols)]
+        held[...] = jnp.dot(hidden[own_seq, early], down_full[s, half, early, lanes], preferred_element_type=f32)
+        when_outer(lambda: extra_copy(mirror, z, partner).wait_recv())
+        product = jnp.dot(hidden[own_seq, late], down_full[s, half, late, lanes], preferred_element_type=f32)
+        part1[j, :, lanes] = (held[...] + product).astype(jnp.bfloat16)
         pair_copy(b).start()
 
     def add_pair(b):
@@ -740,8 +769,8 @@
                 sent(name, z, 1 - g, ysend.at[z], partner).wait_send()
                 for s in (pz, far, mirror):
                     if name != "down":
-                        sent(name, s, g, ysend.at[s], y_peer).wait_send()
-            sent("down", pz, g, ysend.at[pz], y_peer).wait_send()
+                        shared(name, s)
+            shared("down", pz)
             for lane in range(3):
                 lent_all(lane, t).wait_send()
 
@@ -753,7 +782,7 @@
                 sent(name, z, g, zleft, inward).wait_send()
                 sent(name, pz, g, zsend.at[pz], inward).wait_send()
                 for s in (mirror, far):
-                    sent(name, s, g, ysend.at[s], y_peer).wait_send()
+                    shared(name, s)
                     if name != "down":
                         sent(name, s, g, zsend.at[s], partner).wait_send()
             remote(rbuf0, rbuf0, csend.at[0], crecv.at[0, 0], mate).wait_send()
@@ -780,48 +809,52 @@
     when_outer(lambda: settle("down", far))
     multiply(5)
     take_down(mirror, 3, 4)
+    multiply(6)
     add_pair(5)
     finish(0)
+    add_pair(6)
     take_down(mirror, 4, 5)
     drain_early()
     finish(1)
     emit(0)
     take_down(mirror, 5, 6)
+    when_outer(lambda: settle_down(mirror, 0))
+    multiply(7)
     finish(2)
     emit(1)
+    add_pair(7)
     take_down(mirror, 6, 7)
     finish(3)
     emit(2)
-    take_down(mirror, 7, 8)
-    multiply(6)
+    when_outer(lambda: arrival("down", mirror, 7).wait_recv())
+    multiply(8)
+    finish(4)
     emit(3)
-    add_pair(6)
-    finish(4)
-    when_outer(lambda: settle_down(mirror, 0))
-    multiply(7)
+    add_pair(8)
+    multiply_last(9)
     finish(5)
-    add_pair(7)
     emit(4)
-    when_outer(lambda: settle_down(mirror, 1))
-    multiply(8)
+    add_pair(9)
     finish(6)
-    add_pair(8)
     emit(5)
     finish(7)
     emit(6)
     finish(8)
     emit(7)
+    finish(9)
     emit(8)
+    emit(9)
 
     @pl.when(outer)
     def _():
-        for s in (far, mirror):
-            sent("down", s, g, ysend.at[s], y_peer).wait_send()
+        shared("down", far)
+        shared("down", mirror, f_loc // 4 * 3)
 
     @pl.when(inner)
     def _():
         for s in (mirror, far):
             sent("down", s, g, zsend.at[s], partner).wait_send()
+        extra_copy(far, pz, partner).wait_send()
 
     remote(xr1, xr1, csend.at[1], crecv.at[1, 0], mate).wait_send()
     remote(xr1, xr1, xsend.at[1], xrecv.at[1, 0], x_peer).wait_send()
@@ -871,11 +904,11 @@
             vmem((1, width), jnp.float32),
             vmem((1, width), jnp.float32),
             vmem((1, width), jnp.float32),
-            dma((n, 3)), dma((3,)), dma((n - 1, 17)), dma((n, 3)), dma((n - 1, 5)),
+            dma((n, 4)), dma((3,)), dma((n - 1, 17)), dma((n, 4)), dma((n - 1, 6)),
             dma((n_tp - 1,)), dma((n_tp - 1,)), dma((11,)),
             dma((2,)), dma((1 + blocks,)), dma((6,)), dma((5 + blocks,)),
-            dma((2,)), dma((2, blocks + 1)), dma((2,)), dma((2, blocks + 1)), dma((1,)), dma((blocks,)),
-            dma((2,)), dma((2 + blocks,)), dma((1,)),
+            dma((2,)), dma((2, blocks + 2)), dma((2,)), dma((2, blocks + 2)), dma((1,)), dma((blocks,)),
+            dma((2,)), dma((3 + blocks,)), dma((1,)),
         ],
         compiler_params=pltpu.CompilerParams(
             collective_id=0, has_side_effects=True, vmem_limit_bytes=60 * 1024 * 1024

time: 161 us -> 160 us (level)
    pallas_call x1, Pallas kernels: 158 us -> 157 us  [fused_shards(): pl.pallas_call(functools.partial(fused_kernel, (n, n_tp)), out_shape=jax....]
where the time goes in v4:
time: 160 us; the launch traced here: 159 us
  Pallas kernels  157 us (98%)
  local copies, waits for them, and re-layouts  2.73 us (2%)
    pallas_call x1, Pallas kernels, fused_shards(): pl.pallas_call(functools.partial(fused_kernel, (n, n_tp)), out_shape=jax....  157 us

profile of v4, /device:TPU:0, one launch (start us, length us, event | category | flops | bytes accessed | tf_op | source)
XLA Modules:
  0.0 159.2 jit_solution(2019098553407246575)
XLA Ops:
  0.0 156.5 %shard_map.100 = bf16[384,2048]{1,0:T(8,128)(2,1)} custom-call(bf16[384,2048]{1,0:T(8,128)(2,1)} %tok_hbm.1, bf16[512,1280]{1,0:T(8,128)(2,1)} %gate_ref.1, bf16[512,1280]{1,0:T(8,128)(2,1)} %up_ref.1, bf16[1280,512]{1,0:T(8,128)(2,1)} %down_ref.1, bf16[128,4,128]{2,1,0:T(4,128)(2,1)} %pool_hbm.1, f32[4,512]{1,0:T(4,128)} %bias_hbm.1, f32[1,2048]{1,0:T(1,128)} %bitcast.4, ...), custom_call_target="tpu_custom_call" | custom-call | tf_op jit(solution)/shard_map/pallas_call | solution.py:875
  156.5 2.7 %copy.12 = bf16[384,2048]{1,0:T(8,128)(2,1)} copy(bf16[384,2048]{1,0:T(8,128)(2,1)} %shard_map.100) | data formatting | bytes 3145728

commit v5 on v4

--- a/solution.py
+++ b/solution.py
@@ -101,7 +101,7 @@
     gu_full, down_full, pool_full, acc, normed, hidden, amix, res, guest, part0, rbuf0, xs0, xr0, xg0, lent,
     part1, rbuf1, xs1, xr1, tok_ref, pool_ref, bias_ref, scale_ref, gain1_ref, gainm_ref, gain2_ref,
     zsend, zleft, zrecv, ysend, yrecv, tsend, trecv, lsem, asend, arecv, qsend, qrecv,
-    csend, crecv, xsend, xrecv, gsend, grecv, fsend, frecv, osem,
+    csend, crecv, xsend, xrecv, gsend, grecv, fsend, frecv,
 ):
     n, n_tp = sizes
     g, z, t = lax.axis_index("grp"), lax.axis_index("fs"), lax.axis_index("tp")
@@ -695,9 +695,9 @@
         up_proj = jnp.dot(normed[own_seq, :], gu_full[1, :, cols], preferred_element_type=f32)
         hidden[own_seq, cols] = activate(gate_proj, up_proj)
 
-        @pl.when(outer & (i % 2 == 1))
+        @pl.when(outer & ((i == 1) | (i == 2) | (i == 4)))
         def _():
-            take("down", far, 4 + i // 2)
+            take("down", far, 3 + i - i // 4)
 
     def spot(b):
         wide = b < n_blocks - 2
@@ -750,11 +750,12 @@
         total = xs1[j, :, lanes].astype(f32) + xr1[j, :, lanes].astype(f32)
         res[1, mine, cols] = (amix[mine, cols].astype(f32) + 0.5 * total).astype(jnp.bfloat16)
         last_copy(b, mine).start()
+        out_ref[mine, cols] = res[1, mine, cols]
 
     def emit(b):
         cols = spot(b)[2]
         last_copy(b, other).wait_recv()
-        pltpu.make_async_copy(res.at[1, :, cols], out_ref.at[:, cols], osem.at[0]).start()
+        out_ref[other, cols] = res[1, other, cols]
 
     def drain_early():
         for off in range(1, n_tp):
@@ -792,7 +793,6 @@
             final_all(0, mine).wait_send()
 
     multiply(0)
-    take_down(far, 6, 7)
     multiply(1)
     add_pair(0)
     multiply(2)
@@ -822,8 +822,8 @@
     multiply(7)
     finish(2)
     emit(1)
+    take_down(mirror, 6, 7)
     add_pair(7)
-    take_down(mirror, 6, 7)
     finish(3)
     emit(2)
     when_outer(lambda: arrival("down", mirror, 7).wait_recv())
@@ -859,7 +859,6 @@
     remote(xr1, xr1, csend.at[1], crecv.at[1, 0], mate).wait_send()
     remote(xr1, xr1, xsend.at[1], xrecv.at[1, 0], x_peer).wait_send()
     final_all(1, mine).wait_send()
-    pltpu.make_async_copy(res.at[1], out_ref, osem.at[0]).wait()
 
 
 def fused_shards(
@@ -874,9 +873,9 @@
     half, quarter, block, blocks = n_rows // 2, n_rows // n_tp, d_loc // 2, 2 * n
     return pl.pallas_call(
         functools.partial(fused_kernel, (n, n_tp)),
-        out_shape=jax.ShapeDtypeStruct((n_rows, width), bf16),
+        out_shape=pltpu.VMEM((n_rows, width), bf16),
         in_specs=[anywhere] * 10,
-        out_specs=anywhere,
+        out_specs=pl.BlockSpec(memory_space=pltpu.VMEM),
         scratch_shapes=[
             vmem((2, n * d_loc, f_loc), bf16),
             vmem((n, 2, f_loc, block), bf16),
@@ -908,7 +907,7 @@
             dma((n_tp - 1,)), dma((n_tp - 1,)), dma((11,)),
             dma((2,)), dma((1 + blocks,)), dma((6,)), dma((5 + blocks,)),
             dma((2,)), dma((2, blocks + 2)), dma((2,)), dma((2, blocks + 2)), dma((1,)), dma((blocks,)),
-            dma((2,)), dma((3 + blocks,)), dma((1,)),
+            dma((2,)), dma((3 + blocks,)),
         ],
         compiler_params=pltpu.CompilerParams(
             collective_id=0, has_side_effects=True, vmem_limit_bytes=60 * 1024 * 1024

time: 160 us -> 157 us (0.981)
  no operation moved by 1% of the time
where the time goes in v5:
time: 157 us
  Pallas kernels  156 us (99%)
    pallas_call x1, Pallas kernels, fused_shards(): pl.pallas_call(functools.partial(fused_kernel, (n, n_tp)), out_shape=pltp...  156 us

profile of v5, /device:TPU:0, one launch (start us, length us, event | category | flops | bytes accessed | tf_op | source)
XLA Modules:
  0.0 157.2 jit_solution(9387118843178175402)
XLA Ops:
  0.0 156.0 %shard_map.100 = bf16[384,2048]{1,0:T(8,128)(2,1)S(1)} custom-call(bf16[384,2048]{1,0:T(8,128)(2,1)} %tok_hbm.1, bf16[512,1280]{1,0:T(8,128)(2,1)} %gate_ref.1, bf16[512,1280]{1,0:T(8,128)(2,1)} %up_ref.1, bf16[1280,512]{1,0:T(8,128)(2,1)} %down_ref.1, bf16[128,4,128]{2,1,0:T(4,128)(2,1)} %pool_hbm.1, f32[4,512]{1,0:T(4,128)} %bias_hbm.1, ...), custom_call_target="tpu_custom_call" | custom-call | tf_op jit(solution)/shard_map/pallas_call | solution.py:874
  156.1 1.1 copy.12
